TPU v7x, 32 devices: a whole 2x2x4 slice. The times are simulated.
32 devices in a mesh: sp: 8 (over z, x), tp: 4 (over y, core).
Axes of the slice: x: 2, y: 2, z: 4, core: 2. Of those that a mesh axis runs over, the one named last changes fastest.
Arguments:
- resid: bfloat16 [1024, 2048], P('sp'), may hold values from -8 to 8
- a_val: bfloat16 [1024, 1024], P('sp', 'tp'), may hold values from -8 to 8
- a_gate: bfloat16 [1024, 1024], P('sp', 'tp'), may hold values from -6 to 6
- conv_kernel: bfloat16 [31, 1024], P(None, 'tp'), may hold values from -1 to 1
- conv_bias: float32 [1024], P('tp'), may hold values from -3 to 3
- ln_gain: float32 [1024], P('tp'), may hold values from 0.1 to 1.9
- ln_bias: float32 [1024], P('tp'), may hold values from -3 to 3
- w_out: bfloat16 [1024, 2048], P('tp'), may hold values from -0.1875 to 0.1875
- ffn_gain: float32 [2048], replicated, may hold values from 0.1 to 1.9
- routes: int32 [1024, 4], P('sp'), may hold values from 0 to 7, all different within a row; in each aligned block of 128 rows (0 to 127, 128 to 255, ...) at most 128 rows name the same one
- route_weights: float32 [1024, 4], P('sp'), may hold values from 0.15 to 1.2
- exp_gate: bfloat16 [8, 2048, 4096], P('sp', None, 'tp'), may hold values from -0.125 to 0.125
- exp_up: bfloat16 [8, 2048, 4096], P('sp', None, 'tp'), may hold values from -0.125 to 0.125
- exp_down: bfloat16 [8, 4096, 2048], P('sp', None, 'tp'), may hold values from -0.09375 to 0.09375
- sh_gate: bfloat16 [2048, 512], P(None, 'tp'), may hold values from -0.125 to 0.125
- sh_up: bfloat16 [2048, 512], P(None, 'tp'), may hold values from -0.125 to 0.125
- sh_down: bfloat16 [512, 2048], P(None, 'tp'), may hold values from -0.25 to 0.25
Outputs:
- result: bfloat16 [1024, 2048], P('sp', 'tp')
Inputs may be any that keep to these rules, and one draw needn't show every extreme that they name: `routes`: among the 128 rows of one index of sp, each expert is named at most 128 times, a bound that some block reaches; a row names 4 different experts.
All inputs are finite; a program needn't handle non-finite values.
Results may differ from a plain program's by a relative error of at most 0.007.
Values may be sent and summed in bfloat16 or wider, within the bound.
A program may use at most 64 MiB of HBM per device.

v0:
```python
import functools

import jax
import jax.numpy as jnp
from jax import lax
from jax.experimental import pallas as pl
from jax.experimental.pallas import tpu as pltpu
from jax.sharding import PartitionSpec as P

LN_EPS = 1e-05
RMS_EPS = 1e-06


def shifted(value, axis, by):
    size = lax.axis_size(axis)
    pairs = [(i, i + by) for i in range(size) if 0 <= i + by < size]
    return lax.ppermute(value, axis, pairs)


def body_slots(
    resid,
    a_val,
    a_gate,
    conv_kernel,
    conv_bias,
    ln_gain,
    ln_bias,
    w_out,
    ffn_gain,
    routes,
    route_weights,
    exp_gate,
    exp_up,
    exp_down,
    sh_gate,
    sh_up,
    sh_down,
):
    tp_count = lax.axis_size("tp")
    tp_place = lax.axis_index("tp")
    sp_count = lax.axis_size("sp")
    tok_rows = resid.shape[0]
    model_width = resid.shape[1]
    col_width = model_width // tp_count
    col_start = tp_place * col_width
    conv_span = conv_kernel.shape[0]
    channels_all = a_val.shape[1] * tp_count
    gated_in = (a_val.astype(jnp.float32) * jax.nn.sigmoid(a_gate.astype(jnp.float32))).astype(
        jnp.bfloat16
    )
    before = shifted(gated_in[tok_rows - (conv_span - 1) :], "sp", 1)
    padded = jnp.concatenate([before, gated_in], axis=0).astype(jnp.float32)
    kernel = conv_kernel.astype(jnp.float32)

    def add_tap(offset, running):
        window_rows = lax.dynamic_slice_in_dim(padded, offset, tok_rows, 0)
        return running + lax.dynamic_slice_in_dim(kernel, offset, 1, 0) * window_rows

    start_sum = jnp.broadcast_to(conv_bias[None, :], gated_in.shape)
    conv_out = lax.fori_loop(0, conv_span, add_tap, start_sum)
    row_sums = lax.psum((jnp.sum(conv_out, axis=1), jnp.sum(conv_out * conv_out, axis=1)), "tp")
    channel_mean = row_sums[0] / channels_all
    channel_var = row_sums[1] / channels_all - channel_mean * channel_mean
    scaled = (conv_out - channel_mean[:, None]) * lax.rsqrt(
        channel_var[:, None] + LN_EPS
    ) * ln_gain[None, :] + ln_bias[None, :]
    mixed_out = jax.nn.silu(scaled).astype(jnp.bfloat16)
    partial_proj = jnp.dot(mixed_out, w_out, preferred_element_type=jnp.float32)
    projected = lax.psum(partial_proj, "tp")
    middle = (resid.astype(jnp.float32) + projected).astype(jnp.bfloat16)
    middle_f = middle.astype(jnp.float32)
    inverse = lax.rsqrt(jnp.mean(middle_f * middle_f, axis=1, keepdims=True) + RMS_EPS)
    normed = (middle_f * inverse * ffn_gain[None, :]).astype(jnp.bfloat16)
    middle_cols = lax.dynamic_slice_in_dim(middle, col_start, col_width, 1)
    shared_gate = jnp.dot(normed, sh_gate, preferred_element_type=jnp.float32)
    shared_up = jnp.dot(normed, sh_up, preferred_element_type=jnp.float32)
    shared_hidden = (jax.nn.silu(shared_gate) * shared_up).astype(jnp.bfloat16)
    weight_rows = sh_down
    shared = jnp.dot(
        lax.all_gather(shared_hidden, "tp", axis=1, tiled=True),
        weight_rows,
        preferred_element_type=jnp.float32,
    )
    top_count = routes.shape[1]
    local_experts = exp_gate.shape[0]
    experts_all = local_experts * sp_count
    capacity = max(2 * tok_rows * top_count // experts_all, tp_count)
    pair_count = tok_rows * top_count
    chosen = routes.reshape(pair_count)
    one_hot = (chosen[:, None] == jnp.arange(experts_all, dtype=jnp.int32)[None, :]).astype(
        jnp.int32
    )
    earlier = jnp.cumsum(one_hot, axis=0) - one_hot
    place_in = jnp.sum(earlier * one_hot, axis=1)
    slot_of = chosen * capacity + place_in
    owner_ids = (
        jnp.zeros((experts_all * capacity,), jnp.int32)
        .at[slot_of]
        .set(jnp.arange(pair_count, dtype=jnp.int32) + 1)
    )
    owner_grid = owner_ids.reshape(sp_count, local_experts, capacity)
    part_slots = capacity // tp_count
    own_owners = lax.dynamic_slice_in_dim(owner_grid, tp_place * part_slots, part_slots, 2)
    source_row = jnp.maximum(own_owners - 1, 0) // top_count
    taken = normed[source_row.reshape(-1)].reshape(own_owners.shape + (model_width,))
    landed = lax.all_to_all(
        jnp.where((own_owners > 0)[..., None], taken, jnp.zeros((), jnp.bfloat16)),
        "sp",
        split_axis=0,
        concat_axis=0,
        tiled=True,
    )
    arrived = lax.all_gather(landed, "tp", axis=2, tiled=True)
    gate_part = jnp.einsum("sxcd,xdf->sxcf", arrived, exp_gate, preferred_element_type=jnp.float32)
    up_part = jnp.einsum("sxcd,xdf->sxcf", arrived, exp_up, preferred_element_type=jnp.float32)
    expert_hidden = (jax.nn.silu(gate_part) * up_part).astype(jnp.bfloat16)
    weight_rows = exp_down
    expert_sum = jnp.einsum(
        "sxcf,xfd->sxcd",
        lax.all_gather(expert_hidden, "tp", axis=3, tiled=True),
        weight_rows,
        preferred_element_type=jnp.float32,
    )
    expert_out = expert_sum.astype(jnp.bfloat16)
    returned = lax.all_to_all(expert_out, "sp", split_axis=0, concat_axis=0, tiled=True)
    flat_out = returned.reshape(experts_all * capacity, col_width)
    picked = flat_out[slot_of].astype(jnp.float32).reshape(tok_rows, top_count, col_width)
    routed = jnp.sum(picked * route_weights[:, :, None], axis=1)
    return (middle_cols.astype(jnp.float32) + shared + routed).astype(jnp.bfloat16)


def swapped(value, axis, bit):
    size = lax.axis_size(axis)
    return lax.ppermute(value, axis, [(i, i ^ bit) for i in range(size)])


def gather_kernel(
    levels,
    own_ref,
    weight_ref,
    down_ref,
    rows_ref,
    weights_ref,
    swap_ref,
    local_sem,
    up_sem,
    low_sem,
    side_sem,
    core_sem,
    main_recv,
    core_recv,
    weight_send,
    weight_recv,
    swap_sem,
):
    count = 2 * levels
    me = lax.axis_index("sp")
    tp_place = lax.axis_index("tp")
    level, side = me // 2, me % 2
    row, core = tp_place // 2, tp_place % 2
    core_peer = {"tp": row * 2 + (1 - core)}
    row_peer = {"tp": (1 - row) * 2 + core}
    side_peer = {"sp": level * 2 + (1 - side)}
    mesh_ids = pl.DeviceIdType.MESH

    barrier = pltpu.get_barrier_semaphore()
    others = [lax.rem(me + step, count) for step in range(1, count)]
    for other in others:
        pl.semaphore_signal(barrier, inc=1, device_id={"sp": other}, device_id_type=mesh_ids)
    pl.semaphore_signal(barrier, inc=1, device_id=core_peer, device_id_type=mesh_ids)
    pl.semaphore_signal(barrier, inc=1, device_id=row_peer, device_id_type=mesh_ids)
    pl.semaphore_wait(barrier, count + 1)

    def remote(src, dst, send, recv, where):
        return pltpu.make_async_remote_copy(
            src_ref=src, dst_ref=dst, send_sem=send, recv_sem=recv, device_id=where, device_id_type=mesh_ids
        )

    def block(at):
        return rows_ref.at[core, at]

    half_rows = swap_ref.shape[0]
    swap = remote(
        down_ref.at[0, pl.ds(pl.multiple_of((1 - row) * half_rows, half_rows), half_rows)],
        swap_ref,
        swap_sem.at[0],
        swap_sem.at[1],
        row_peer,
    )

    def up_copy(src, origin):
        at = origin * 2 + side
        return remote(src, block(at), up_sem.at[origin], main_recv.at[at], {"sp": me + 2})

    def low_copy(src, origin):
        at = origin * 2 + side
        return remote(src, block(at), low_sem.at[origin], main_recv.at[at], {"sp": me - 2})

    def side_copy(src, origin):
        at = origin * 2 + side
        return remote(src, block(at), side_sem.at[origin], main_recv.at[at], side_peer)

    def core_copy(src, at):
        return remote(src, block(at), core_sem.at[at], core_recv.at[at], core_peer)

    def landed(at):
        remote(block(at), block(at), core_sem.at[at], main_recv.at[at], core_peer).wait_recv()

    @pl.when(level < levels - 1)
    def _():
        up_copy(own_ref, level).start()

    @pl.when(level > 0)
    def _():
        low_copy(own_ref, level).start()

    side_copy(own_ref, level).start()
    swap.start()
    core_copy(own_ref, me).start()
    weight_copies = [
        remote(
            weight_ref,
            weights_ref.at[me],
            weight_send.at[step],
            weight_recv.at[me],
            {"sp": other},
        )
        for step, other in enumerate(others)
    ]
    for copy in weight_copies:
        copy.start()
    keep = pltpu.make_async_copy(own_ref, block(me), local_sem.at[0])
    keep.start()
    keep_weight = pltpu.make_async_copy(weight_ref, weights_ref.at[me], local_sem.at[1])
    keep_weight.start()

    for step in range(1, levels):
        below = level - step
        above = level + step

        @pl.when(below >= 0)
        def _():
            at = below * 2 + side
            landed(at)

            @pl.when(level < levels - 1)
            def _():
                up_copy(block(at), below).start()

            side_copy(block(at), below).start()
            core_copy(block(at), at).start()

        @pl.when(above < levels)
        def _():
            at = above * 2 + side
            landed(at)

            @pl.when(level > 0)
            def _():
                low_copy(block(at), above).start()

            side_copy(block(at), above).start()
            core_copy(block(at), at).start()

    def from_side(origin):
        at = origin * 2 + (1 - side)
        landed(at)
        core_copy(block(at), at).start()

    from_side(level)
    for step in range(1, levels):
        below = level - step
        above = level + step

        @pl.when(below >= 0)
        def _():
            from_side(below)

        @pl.when(above < levels)
        def _():
            from_side(above)

    keep.wait()
    keep_weight.wait()
    for copy in weight_copies:
        copy.wait_send()
    for other in others:
        remote(
            weight_ref, weights_ref.at[other], weight_send.at[0], weight_recv.at[other], core_peer
        ).wait_recv()
    for origin in range(levels):
        side_copy(own_ref, origin).wait_send()

        @pl.when((level < levels - 1) & (origin <= level))
        def _():
            up_copy(own_ref, origin).wait_send()

        @pl.when((level > 0) & (origin >= level))
        def _():
            low_copy(own_ref, origin).wait_send()

    for at in range(count):
        core_copy(own_ref, at).wait_send()
        far = rows_ref.at[1 - core, at]
        remote(far, far, core_sem.at[at], core_recv.at[at], core_peer).wait_recv()
    swap.wait()


def gather_rows(mid_half, weight_rows, down, half_rows):
    count = lax.axis_size("sp")
    levels = count // 2
    tok_rows, half_width = mid_half.shape
    vmem = pl.BlockSpec(memory_space=pltpu.VMEM)
    hbm = pl.BlockSpec(memory_space=pltpu.HBM)
    dma = pltpu.SemaphoreType.DMA
    return pl.pallas_call(
        functools.partial(gather_kernel, levels),
        out_shape=(
            jax.ShapeDtypeStruct((2, count, tok_rows, half_width), mid_half.dtype),
            jax.ShapeDtypeStruct((count,) + weight_rows.shape, weight_rows.dtype),
            jax.ShapeDtypeStruct((half_rows, down.shape[2]), down.dtype),
        ),
        in_specs=[vmem, vmem, hbm],
        out_specs=(vmem, vmem, hbm),
        scratch_shapes=[
            dma((2,)),
            dma((levels,)),
            dma((levels,)),
            dma((levels,)),
            dma((count,)),
            dma((count,)),
            dma((count,)),
            dma((count - 1,)),
            dma((count,)),
            dma((2,)),
        ],
        compiler_params=pltpu.CompilerParams(
            collective_id=0, has_side_effects=True, vmem_limit_bytes=24 * 1024 * 1024
        ),
    )(mid_half, weight_rows, down)


def body_dense(
    resid,
    a_val,
    a_gate,
    conv_kernel,
    conv_bias,
    ln_gain,
    ln_bias,
    w_out,
    ffn_gain,
    routes,
    route_weights,
    exp_gate,
    exp_up,
    exp_down,
    sh_gate,
    sh_up,
    sh_down,
):
    tp_count = lax.axis_size("tp")
    tp_place = lax.axis_index("tp")
    core = tp_place % 2
    row = tp_place // 2
    sp_count = lax.axis_size("sp")
    tok_rows, model_width = resid.shape
    col_width = model_width // tp_count
    half_width = model_width // 2
    part_hidden = exp_gate.shape[2]
    conv_span = conv_kernel.shape[0]
    channels_all = a_val.shape[1] * tp_count

    gated_in = (a_val.astype(jnp.float32) * jax.nn.sigmoid(a_gate.astype(jnp.float32))).astype(
        jnp.bfloat16
    )
    before = shifted(gated_in[tok_rows - (conv_span - 1) :], "sp", 1)
    expert_ids = jnp.arange(sp_count, dtype=jnp.int32)
    weight_mat = jnp.sum(
        jnp.where(routes[:, :, None] == expert_ids[None, None, :], route_weights[:, :, None], 0.0),
        axis=1,
    )
    padded = jnp.concatenate([before, gated_in], axis=0).astype(jnp.float32)
    kernel = conv_kernel.astype(jnp.float32)
    conv_out = jnp.broadcast_to(conv_bias[None, :], gated_in.shape)
    for tap in range(conv_span):
        conv_out = conv_out + kernel[tap : tap + 1] * padded[tap : tap + tok_rows]
    row_sums = lax.psum((jnp.sum(conv_out, axis=1), jnp.sum(conv_out * conv_out, axis=1)), "tp")
    channel_mean = row_sums[0] / channels_all
    channel_var = row_sums[1] / channels_all - channel_mean * channel_mean
    scaled = (conv_out - channel_mean[:, None]) * lax.rsqrt(
        channel_var[:, None] + LN_EPS
    ) * ln_gain[None, :] + ln_bias[None, :]
    mixed_out = jax.nn.silu(scaled).astype(jnp.bfloat16)
    partial_proj = jnp.dot(mixed_out, w_out, preferred_element_type=jnp.float32)
    give = lax.dynamic_slice_in_dim(partial_proj, (1 - core) * half_width, half_width, 1)
    keep = lax.dynamic_slice_in_dim(partial_proj, core * half_width, half_width, 1)
    chip_sum = keep + swapped(give.astype(jnp.bfloat16), "tp", 1).astype(jnp.float32)
    chip_sum = chip_sum.astype(jnp.bfloat16)
    half_sum = chip_sum.astype(jnp.float32) + swapped(chip_sum, "tp", 2).astype(jnp.float32)
    resid_half = lax.dynamic_slice_in_dim(resid, core * half_width, half_width, 1)
    mid_half = (resid_half.astype(jnp.float32) + half_sum).astype(jnp.bfloat16)
    gathered, weights_got, swapped_down = gather_rows(
        mid_half, weight_mat.T, exp_down, 2 * part_hidden
    )
    sp_place = lax.axis_index("sp")
    weight_own = lax.dynamic_index_in_dim(weights_got, sp_place, 1, False).reshape(-1, 1)
    own_halves = lax.dynamic_index_in_dim(gathered, sp_place, 1, False)
    middle = jnp.concatenate([own_halves[0], own_halves[1]], axis=1)

    middle_f = middle.astype(jnp.float32)
    inverse = lax.rsqrt(jnp.mean(middle_f * middle_f, axis=1, keepdims=True) + RMS_EPS)
    normed = (middle_f * inverse * ffn_gain[None, :]).astype(jnp.bfloat16)
    middle_cols = lax.dynamic_slice_in_dim(middle, tp_place * col_width, col_width, 1)
    shared_gate = jnp.dot(normed, sh_gate, preferred_element_type=jnp.float32)
    shared_up = jnp.dot(normed, sh_up, preferred_element_type=jnp.float32)
    shared_hidden = (jax.nn.silu(shared_gate) * shared_up).astype(jnp.bfloat16)
    shared = jnp.dot(
        lax.all_gather(shared_hidden, "tp", axis=1, tiled=True),
        sh_down,
        preferred_element_type=jnp.float32,
    )

    all_rows = sp_count * tok_rows
    rows_f = jnp.concatenate(
        [gathered[0].reshape(all_rows, half_width), gathered[1].reshape(all_rows, half_width)], axis=1
    ).astype(jnp.float32)
    rows_inverse = lax.rsqrt(jnp.mean(rows_f * rows_f, axis=1, keepdims=True) + RMS_EPS)
    rows = (rows_f * rows_inverse * ffn_gain[None, :]).astype(jnp.bfloat16)
    gate_part = jnp.dot(rows, exp_gate[0], preferred_element_type=jnp.float32)
    up_part = jnp.dot(rows, exp_up[0], preferred_element_type=jnp.float32)
    hidden = (jax.nn.silu(gate_part) * up_part).astype(jnp.bfloat16)
    hidden_peer = swapped(hidden, "tp", 1)

    own_at = tp_place * part_hidden
    peer_at = (tp_place ^ 1) * part_hidden
    stay = lax.dynamic_slice_in_dim
    out_far = jnp.dot(
        hidden, stay(swapped_down, core * part_hidden, part_hidden, 0), preferred_element_type=jnp.float32
    ) + jnp.dot(
        hidden_peer,
        stay(swapped_down, (1 - core) * part_hidden, part_hidden, 0),
        preferred_element_type=jnp.float32,
    )
    far = swapped((out_far * weight_own).astype(jnp.bfloat16), "tp", 2)
    out_own = jnp.dot(
        hidden, stay(exp_down[0], own_at, part_hidden, 0), preferred_element_type=jnp.float32
    ) + jnp.dot(
        hidden_peer, stay(exp_down[0], peer_at, part_hidden, 0), preferred_element_type=jnp.float32
    )
    expert_sum = (out_own * weight_own + far.astype(jnp.float32)).astype(jnp.bfloat16)
    returned = lax.all_to_all(
        expert_sum.reshape(sp_count, tok_rows, col_width), "sp", split_axis=0, concat_axis=0, tiled=True
    )
    routed = jnp.sum(returned.astype(jnp.float32), axis=0)
    return (middle_cols.astype(jnp.float32) + shared + routed).astype(jnp.bfloat16)


def body(*args):
    tok_rows = args[0].shape[0]
    top_count = args[9].shape[1]
    local_experts = args[11].shape[0]
    experts_all = local_experts * lax.axis_size("sp")
    capacity = 2 * tok_rows * top_count // experts_all
    if (
        local_experts == 1
        and lax.axis_size("tp") == 4
        and lax.axis_size("sp") % 2 == 0
        and capacity >= tok_rows
    ):
        return body_dense(*args)
    return body_slots(*args)


def solution(mesh):
    in_specs = (
        P("sp", None),
        P("sp", "tp"),
        P("sp", "tp"),
        P(None, "tp"),
        P("tp"),
        P("tp"),
        P("tp"),
        P("tp", None),
        P(),
        P("sp", None),
        P("sp", None),
        P("sp", None, "tp"),
        P("sp", None, "tp"),
        P("sp", None, "tp"),
        P(None, "tp"),
        P(None, "tp"),
        P(None, "tp"),
    )
    out_specs = P("sp", "tp")
    return jax.shard_map(body, mesh=mesh, in_specs=in_specs, out_specs=out_specs, check_vma=False)
```

profile of v0, /device:TPU:0, one launch (start us, length us, event | category | flops | bytes accessed | tf_op | source)
XLA Modules:
  0.0 160.5 jit_solution(16360836745069250348)
XLA Ops:
  0.0 0.0 copy-start
  0.0 0.0 copy-start.7
  0.0 0.0 copy-start.8
  0.0 1.0 multiply_convert_fusion.3
  1.0 4.9 %collective-permute-start = (bf16[30,256]{1,0:T(8,128)(2,1)S(1)}, bf16[30,256]{1,0:T(8,128)(2,1)S(1)}, u32[]{:S(2)}, u32[]{:S(2)}) collective-permute-start(bf16[30,256]{1,0:T(8,128)(2,1)S(1)} %slice.271), channel_id=1, source_target_pairs={{0,4},{4,8},{8,12},{12,16},{16,20},{20,24},{24,28},{1,5},{5,9},{9,... | collective-permute-start | bytes 46088 | tf_op jit(solution)/shard_map/ppermute | solution.py:17
  5.9 1.0 fusion.75
  6.9 1.0 fusion.76
  7.9 0.0 copy-start.5
  7.9 0.0 copy-start.6
  7.9 0.0 copy-start.4
  8.0 0.0 collective-permute-done
  8.0 1.3 fusion.72
  9.3 6.3 %all-reduce = (f32[128]{0:T(128)S(1)}, f32[128]{0:T(128)S(1)}) all-reduce(f32[128]{0:T(128)S(1)} %get-tuple-element.12, f32[128]{0:T(128)S(1)} %get-tuple-element.11), channel_id=1, replica_groups=mesh['sp'=8,'tp'=4] {'tp'}, use_global_device_ids=true, to_apply=%region_3.4 | all-reduce | flops 256 | bytes 2048 | tf_op jit(solution)/shard_map/psum | solution.py:388
  15.7 0.0 copy-done
  15.7 0.0 copy-done.7
  15.7 0.0 copy-done.8
  15.7 0.4 fusion.56
  16.1 0.1 collective-permute-start.1
  16.2 1.5 collective-permute-done.1
  17.7 0.1 add_convert_fusion.2
  17.8 1.1 collective-permute-start.2
  18.9 0.0 copy-done.5
  18.9 0.0 copy-done.6
  18.9 7.3 %collective-permute-done.2 = bf16[128,1024]{1,0:T(8,128)(2,1)S(1)} collective-permute-done((bf16[128,1024]{1,0:T(8,128)(2,1)S(1)}, bf16[128,1024]{1,0:T(8,128)(2,1)S(1)}, u32[]{:S(2)}, u32[]{:S(2)}) %collective-permute-start.2) | collective-permute-done | bytes 262176 | tf_op jit(solution)/shard_map/ppermute | solution.py:134
  26.2 0.0 copy-done.4
  26.2 0.1 add_convert_fusion.1.own_ref
  26.3 0.0 copy-start.2
  26.4 2.2 %copy-done.2 = bf16[1,4096,512]{2,1,0:T(8,128)(2,1)S(1)} copy-done((bf16[1,4096,512]{2,1,0:T(8,128)(2,1)S(1)}, bf16[1,4096,512]{2,1,0:T(8,128)(2,1)}, u32[]{:S(2)}) %copy-start.2) | copy-done | bytes 4194328
  28.5 51.0 %shard_map.163 = (bf16[2,8,128,1024]{3,2,1,0:T(8,128)(2,1)S(1)}, f32[8,8,128]{2,1,0:T(8,128)S(1)}, bf16[2048,512]{1,0:T(8,128)(2,1)S(1)}) custom-call(bf16[128,1024]{1,0:T(8,128)(2,1)S(1)} %add_convert_fusion.1.own_ref, f32[8,128]{1,0:T(8,128)S(1)} %bitcast.63, bf16[1,4096,512]{2,1,0:T(8,128)(2,1)S(1)} %copy-done.2), custom_call_target="tpu_custom_call" | custom-call | tf_op jit(solution)/shard_map/pallas_call | solution.py:316
  79.5 0.0 copy-start.1
  79.5 0.6 fusion.74
  80.1 1.5 copy-done.1
  81.6 0.0 copy-start.9
  81.6 0.0 copy-start.11
  81.6 1.0 fusion
  82.6 1.2 copy-done.9
  83.8 0.0 copy-done.11
  83.8 0.0 copy-start.10
  83.8 4.6 %fusion.3 = f32[1024,1024]{1,0:T(8,128)S(1)} fusion(bf16[1,2048,1024]{2,1,0:T(8,128)(2,1)S(1)} %copy-done.9, f32[2048]{0:T(1024)S(1)} %copy-done.11, f32[1024]{0:T(1024)S(1)} %add_rsqrt_fusion, bf16[1024,1024]{1,0:T(8,128)(2,1)S(1)} %bitcast.68, bf16[1024,1024]{1,0:T(8,128)(2,1)S(1)} %bitcast.65), kind=kOutput, calls=%fused_computation.6 | convolution fusion | flops 4309647360 | bytes 12595200 | tf_op jit(solution)/shard_map/dot_general | solution.py:431
  88.4 0.0 copy-done.10
  88.4 6.6 %multiply_convert_fusion = bf16[1024,1024]{1,0:T(8,128)(2,1)} fusion(f32[1024,1024]{1,0:T(8,128)S(1)} %fusion.3, bf16[1,2048,1024]{2,1,0:T(8,128)(2,1)S(1)} %copy-done.10, f32[2048]{0:T(1024)S(1)} %copy-done.11, f32[1024]{0:T(1024)S(1)} %add_rsqrt_fusion, bf16[1024,1024]{1,0:T(8,128)(2,1)S(1)} %bitcast.69, bf16[1024,1024]{1,0:T(8,128)(2,1)S(1)} %bitcast.66), kind=kOutput, calls=%fused_computation.10 | convolution fusion | flops 4315938816 | bytes 14692352 | tf_op jit(solution)/shard_map/dot_general | solution.py:430
  95.0 0.0 collective-permute-start.3
  95.0 2.8 %fusion.20 = f32[1024,512]{1,0:T(8,128)S(1)} fusion(bf16[1024,1024]{1,0:T(8,128)(2,1)} %multiply_convert_fusion, bf16[2048,512]{1,0:T(8,128)(2,1)S(1)} %get-tuple-element.10, s32[]{:T(128)S(6)} %select_n.36), kind=kOutput, calls=%fused_computation.29 | convolution fusion | flops 1073741824 | bytes 5242884 | tf_op jit(solution)/shard_map/dot_general | solution.py:438
  97.9 1.6 %collective-permute-done.3 = bf16[1024,1024]{1,0:T(8,128)(2,1)} collective-permute-done((bf16[1024,1024]{1,0:T(8,128)(2,1)}, bf16[1024,1024]{1,0:T(8,128)(2,1)}, u32[]{:S(2)}, u32[]{:S(2)}) %collective-permute-start.3) | collective-permute-done | bytes 2097184 | tf_op jit(solution)/shard_map/ppermute | solution.py:134
  99.5 3.9 %multiply_convert_fusion.1 = bf16[1024,512]{1,0:T(8,128)(2,1)} fusion(f32[1024,512]{1,0:T(8,128)S(1)} %fusion.20, bf16[1024,1024]{1,0:T(8,128)(2,1)} %collective-permute-done.3, bf16[2048,512]{1,0:T(8,128)(2,1)S(1)} %get-tuple-element.10, s32[]{:T(128)S(6)} %select_n.37, f32[1024]{0:T(1024)S(1)} %bitcast.70), kind=kOutput, calls=%fused_computation.13 | convolution fusion | flops 1075314688 | bytes 6295556 | tf_op jit(solution)/shard_map/dot_general | solution.py:440
  103.4 0.3 collective-permute-start.4
  103.7 3.1 %fusion.17 = f32[1024,512]{1,0:T(8,128)S(1)} fusion(bf16[1024,1024]{1,0:T(8,128)(2,1)} %multiply_convert_fusion, bf16[1,4096,512]{2,1,0:T(8,128)(2,1)} %down_ref.1, s32[]{:T(128)S(6)} %select_n.41), kind=kOutput, calls=%fused_computation.26 | convolution fusion | flops 1073741824 | bytes 5242884 | tf_op jit(solution)/shard_map/dot_general | solution.py:446
  106.8 3.1 %fusion.15 = f32[1024,512]{1,0:T(8,128)S(1)} fusion(bf16[1024,1024]{1,0:T(8,128)(2,1)} %collective-permute-done.3, bf16[1,4096,512]{2,1,0:T(8,128)(2,1)} %down_ref.1, s32[]{:T(128)S(6)} %select_n.42), kind=kOutput, calls=%fused_computation.24 | convolution fusion | flops 1073741824 | bytes 5242884 | tf_op jit(solution)/shard_map/dot_general | solution.py:448
  109.9 18.9 %collective-permute-done.4 = bf16[1024,512]{1,0:T(8,128)(2,1)S(1)} collective-permute-done((bf16[1024,512]{1,0:T(8,128)(2,1)}, bf16[1024,512]{1,0:T(8,128)(2,1)S(1)}, u32[]{:S(2)}, u32[]{:S(2)}) %collective-permute-start.4) | collective-permute-done | bytes 1048608 | tf_op jit(solution)/shard_map/ppermute | solution.py:134
  128.8 1.4 add_convert_fusion
  130.2 0.0 copy-start.3
  130.2 3.7 %all-to-all-start = ((bf16[8,128,512]{2,1,0:T(8,128)(2,1)}), bf16[8,128,512]{2,1,0:T(8,128)(2,1)S(1)}, u32[]{:S(2)}, u32[]{:S(2)}) async-start(bf16[8,128,512]{2,1,0:T(8,128)(2,1)} %bitcast.41), calls=%async_computation | async-start | bytes 2097152 | tf_op jit(solution)/shard_map/all_to_all | solution.py:452
  133.9 1.1 dynamic-slice_bitcast_fusion.1
  135.0 0.2 fusion.12
  135.2 1.4 fusion.68
  136.6 1.4 fusion.11
  138.0 5.4 %all_gather.3 = bf16[128,512]{1,0:T(8,128)(2,1)S(1)} all-gather(bf16[128,128]{1,0:T(8,128)(2,1)S(1)} %fusion.11), channel_id=1, replica_groups=mesh['sp'=8,'tp'=4] {'tp'}, dimensions={1}, use_global_device_ids=true | all-gather | bytes 163840 | tf_op jit(solution)/shard_map/all_gather | solution.py:419
  143.5 16.0 %all-to-all-done = bf16[8,128,512]{2,1,0:T(8,128)(2,1)S(1)} async-done(((bf16[8,128,512]{2,1,0:T(8,128)(2,1)}), bf16[8,128,512]{2,1,0:T(8,128)(2,1)S(1)}, u32[]{:S(2)}, u32[]{:S(2)}) %all-to-all-start) | async-done | bytes 1048608 | tf_op jit(solution)/shard_map/all_to_all | solution.py:452
  159.4 0.1 convert_reduce_fusion
  159.6 0.0 copy-done.3
  159.6 0.9 fusion.10
  (8 shorter events, 0.1 us)
Async XLA Ops:
  0.0 15.7 %copy-start = (bf16[256,2048]{1,0:T(8,128)(2,1)S(1)}, bf16[256,2048]{1,0:T(8,128)(2,1)}, u32[]{:S(2)}) copy-start(bf16[256,2048]{1,0:T(8,128)(2,1)} %param.24) | copy-start | bytes 3145732
  0.0 15.7 %copy-start.7 = (f32[256]{0:T(256)S(1)}, f32[256]{0:T(256)}, u32[]{:S(2)}) copy-start(f32[256]{0:T(256)} %param.23) | copy-start | bytes 3076
  0.0 15.7 %copy-start.8 = (f32[256]{0:T(256)S(1)}, f32[256]{0:T(256)}, u32[]{:S(2)}) copy-start(f32[256]{0:T(256)} %param.22) | copy-start | bytes 3076
  1.0 6.9 %collective-permute-start = (bf16[30,256]{1,0:T(8,128)(2,1)S(1)}, bf16[30,256]{1,0:T(8,128)(2,1)S(1)}, u32[]{:S(2)}, u32[]{:S(2)}) collective-permute-start(bf16[30,256]{1,0:T(8,128)(2,1)S(1)} %slice.271), channel_id=1, source_target_pairs={{0,4},{4,8},{8,12},{12,16},{16,20},{20,24},{24,28},{1,5},{5,9},{9,... | collective-permute-start | bytes 46088 | tf_op jit(solution)/shard_map/ppermute | solution.py:17
  7.9 11.0 %copy-start.5 = (f32[128,4]{0,1:T(4,128)S(1)}, f32[128,4]{0,1:T(4,128)}, u32[]{:S(2)}) copy-start(f32[128,4]{0,1:T(4,128)} %param.27) | copy-start | bytes 6148
  7.9 11.0 %copy-start.6 = (s32[128,4]{0,1:T(4,128)S(1)}, s32[128,4]{0,1:T(4,128)}, u32[]{:S(2)}) copy-start(s32[128,4]{0,1:T(4,128)} %param.26) | copy-start | bytes 6148
  7.9 18.3 %copy-start.4 = (bf16[128,2048]{1,0:T(8,128)(2,1)S(1)}, bf16[128,2048]{1,0:T(8,128)(2,1)}, u32[]{:S(2)}) copy-start(bf16[128,2048]{1,0:T(8,128)(2,1)} %param.17) | copy-start | bytes 1572868
  16.1 1.6 collective-permute-start.1
  17.8 8.4 %collective-permute-start.2 = (bf16[128,1024]{1,0:T(8,128)(2,1)S(1)}, bf16[128,1024]{1,0:T(8,128)(2,1)S(1)}, u32[]{:S(2)}, u32[]{:S(2)}) collective-permute-start(bf16[128,1024]{1,0:T(8,128)(2,1)S(1)} %add_convert_fusion.2), channel_id=1, source_target_pairs={{0,2},{1,3},{2,0},{3,1},{4,6},{5,7},{6,4},{7,5},{8,10},{9,11},{10,... | collective-permute-start | bytes 786440 | tf_op jit(solution)/shard_map/ppermute | solution.py:134
  26.3 2.2 %copy-start.2 = (bf16[1,4096,512]{2,1,0:T(8,128)(2,1)S(1)}, bf16[1,4096,512]{2,1,0:T(8,128)(2,1)}, u32[]{:S(2)}) copy-start(bf16[1,4096,512]{2,1,0:T(8,128)(2,1)} %down_ref.1) | copy-start | bytes 12582916
  79.5 2.1 %copy-start.1 = (bf16[2,8,128,1024]{3,2,1,0:T(8,128)(2,1)}, bf16[2,8,128,1024]{3,2,1,0:T(8,128)(2,1)S(1)}, u32[]{:S(2)}) copy-start(bf16[2,8,128,1024]{3,2,1,0:T(8,128)(2,1)S(1)} %get-tuple-element.8) | copy-start | bytes 12582916
  81.6 2.2 %copy-start.9 = (bf16[1,2048,1024]{2,1,0:T(8,128)(2,1)S(1)}, bf16[1,2048,1024]{2,1,0:T(8,128)(2,1)}, u32[]{:S(2)}) copy-start(bf16[1,2048,1024]{2,1,0:T(8,128)(2,1)} %param.29) | copy-start | bytes 12582916
  81.6 2.2 %copy-start.11 = (f32[2048]{0:T(1024)S(1)}, f32[2048]{0:T(1024)}, u32[]{:S(2)}) copy-start(f32[2048]{0:T(1024)} %param.25) | copy-start | bytes 24580
  83.8 4.6 %copy-start.10 = (bf16[1,2048,1024]{2,1,0:T(8,128)(2,1)S(1)}, bf16[1,2048,1024]{2,1,0:T(8,128)(2,1)}, u32[]{:S(2)}) copy-start(bf16[1,2048,1024]{2,1,0:T(8,128)(2,1)} %param.28) | copy-start | bytes 12582916
  95.0 4.5 %collective-permute-start.3 = (bf16[1024,1024]{1,0:T(8,128)(2,1)}, bf16[1024,1024]{1,0:T(8,128)(2,1)}, u32[]{:S(2)}, u32[]{:S(2)}) collective-permute-start(bf16[1024,1024]{1,0:T(8,128)(2,1)} %multiply_convert_fusion), channel_id=1, source_target_pairs={{0,1},{1,0},{2,3},{3,2},{4,5},{5,4},{6,7},{7,6},{8,9},{9,8},{10,11... | collective-permute-start | bytes 6291464 | tf_op jit(solution)/shard_map/ppermute | solution.py:134
  103.4 25.4 %collective-permute-start.4 = (bf16[1024,512]{1,0:T(8,128)(2,1)}, bf16[1024,512]{1,0:T(8,128)(2,1)S(1)}, u32[]{:S(2)}, u32[]{:S(2)}) collective-permute-start(bf16[1024,512]{1,0:T(8,128)(2,1)} %multiply_convert_fusion.1), channel_id=1, source_target_pairs={{0,2},{1,3},{2,0},{3,1},{4,6},{5,7},{6,4},{7,5},{8,10},{9,11},{10,... | collective-permute-start | bytes 3145736 | tf_op jit(solution)/shard_map/ppermute | solution.py:134
  130.2 29.4 %copy-start.3 = (bf16[512,512]{1,0:T(8,128)(2,1)S(1)}, bf16[512,512]{1,0:T(8,128)(2,1)}, u32[]{:S(2)}) copy-start(bf16[512,512]{1,0:T(8,128)(2,1)} %param.33) | copy-start | bytes 1572868
  130.2 29.2 %all-to-all-start = ((bf16[8,128,512]{2,1,0:T(8,128)(2,1)}), bf16[8,128,512]{2,1,0:T(8,128)(2,1)S(1)}, u32[]{:S(2)}, u32[]{:S(2)}) async-start(bf16[8,128,512]{2,1,0:T(8,128)(2,1)} %bitcast.41), calls=%async_computation | async-start | bytes 2097152 | tf_op jit(solution)/shard_map/all_to_all | solution.py:452
where the time goes:
time: 161 us
  Pallas kernels  51 us (32%)
  waiting for transfers between devices  45.3 us (28%)
  matrix products  28.2 us (18%)
  blocking collectives  11.8 us (7%)
  starting transfers between devices  10.1 us (6%)
  local copies, waits for them, and re-layouts  8.6 us (5%)
  other arithmetic  5.25 us (3%)
    pallas_call x1, Pallas kernels, gather_rows(): pl.pallas_call(functools.partial(gather_kernel, levels), out_shape=(jax.S...  51 us
    ppermute x4, waiting for transfers between devices, swapped(): return lax.ppermute(value, axis, [(i, i ^ bit) for i in range(size)])  29.4 us
    all_to_all x1, waiting for transfers between devices, body_dense(): lax.all_to_all(expert_sum.reshape(sp_count, tok_rows, col_width), 'sp', s...  16 us
    dot_general x1, matrix products, body_dense(): gate_part = jnp.dot(rows, exp_gate[0], preferred_element_type=jnp.float32)  6.63 us
    psum x1, blocking collectives, body_dense(): lax.psum((jnp.sum(conv_out, axis=1), jnp.sum(conv_out * conv_out, axis=1)...  6.33 us
    all_gather x1, blocking collectives, body_dense(): lax.all_gather(shared_hidden, 'tp', axis=1, tiled=True)  5.45 us
    unnamed x24, local copies, waits for them, and re-layouts  4.89 us
    ppermute x1, starting transfers between devices, shifted(): return lax.ppermute(value, axis, pairs)  4.88 us
  transfers between devices with their start and end apart: 6, of which 5 were waited for; matrix products, arithmetic and copies ran while one was open for 9% of the time, Pallas kernels for 0%

commit v1 on v0

v1 whole, which is shorter than its diff:
```python
import functools

import jax
import jax.numpy as jnp
from jax import lax
from jax.experimental import pallas as pl
from jax.experimental.pallas import tpu as pltpu
from jax.sharding import PartitionSpec as P

LN_EPS = 1e-05
RMS_EPS = 1e-06


def shifted(value, axis, by):
    size = lax.axis_size(axis)
    pairs = [(i, i + by) for i in range(size) if 0 <= i + by < size]
    return lax.ppermute(value, axis, pairs)


def body_slots(
    resid,
    a_val,
    a_gate,
    conv_kernel,
    conv_bias,
    ln_gain,
    ln_bias,
    w_out,
    ffn_gain,
    routes,
    route_weights,
    exp_gate,
    exp_up,
    exp_down,
    sh_gate,
    sh_up,
    sh_down,
):
    tp_count = lax.axis_size("tp")
    tp_place = lax.axis_index("tp")
    sp_count = lax.axis_size("sp")
    tok_rows = resid.shape[0]
    model_width = resid.shape[1]
    col_width = model_width // tp_count
    col_start = tp_place * col_width
    conv_span = conv_kernel.shape[0]
    channels_all = a_val.shape[1] * tp_count
    gated_in = (a_val.astype(jnp.float32) * jax.nn.sigmoid(a_gate.astype(jnp.float32))).astype(
        jnp.bfloat16
    )
    before = shifted(gated_in[tok_rows - (conv_span - 1) :], "sp", 1)
    padded = jnp.concatenate([before, gated_in], axis=0).astype(jnp.float32)
    kernel = conv_kernel.astype(jnp.float32)

    def add_tap(offset, running):
        window_rows = lax.dynamic_slice_in_dim(padded, offset, tok_rows, 0)
        return running + lax.dynamic_slice_in_dim(kernel, offset, 1, 0) * window_rows

    start_sum = jnp.broadcast_to(conv_bias[None, :], gated_in.shape)
    conv_out = lax.fori_loop(0, conv_span, add_tap, start_sum)
    row_sums = lax.psum((jnp.sum(conv_out, axis=1), jnp.sum(conv_out * conv_out, axis=1)), "tp")
    channel_mean = row_sums[0] / channels_all
    channel_var = row_sums[1] / channels_all - channel_mean * channel_mean
    scaled = (conv_out - channel_mean[:, None]) * lax.rsqrt(
        channel_var[:, None] + LN_EPS
    ) * ln_gain[None, :] + ln_bias[None, :]
    mixed_out = jax.nn.silu(scaled).astype(jnp.bfloat16)
    partial_proj = jnp.dot(mixed_out, w_out, preferred_element_type=jnp.float32)
    projected = lax.psum(partial_proj, "tp")
    middle = (resid.astype(jnp.float32) + projected).astype(jnp.bfloat16)
    middle_f = middle.astype(jnp.float32)
    inverse = lax.rsqrt(jnp.mean(middle_f * middle_f, axis=1, keepdims=True) + RMS_EPS)
    normed = (middle_f * inverse * ffn_gain[None, :]).astype(jnp.bfloat16)
    middle_cols = lax.dynamic_slice_in_dim(middle, col_start, col_width, 1)
    shared_gate = jnp.dot(normed, sh_gate, preferred_element_type=jnp.float32)
    shared_up = jnp.dot(normed, sh_up, preferred_element_type=jnp.float32)
    shared_hidden = (jax.nn.silu(shared_gate) * shared_up).astype(jnp.bfloat16)
    weight_rows = sh_down
    shared = jnp.dot(
        lax.all_gather(shared_hidden, "tp", axis=1, tiled=True),
        weight_rows,
        preferred_element_type=jnp.float32,
    )
    top_count = routes.shape[1]
    local_experts = exp_gate.shape[0]
    experts_all = local_experts * sp_count
    capacity = max(2 * tok_rows * top_count // experts_all, tp_count)
    pair_count = tok_rows * top_count
    chosen = routes.reshape(pair_count)
    one_hot = (chosen[:, None] == jnp.arange(experts_all, dtype=jnp.int32)[None, :]).astype(
        jnp.int32
    )
    earlier = jnp.cumsum(one_hot, axis=0) - one_hot
    place_in = jnp.sum(earlier * one_hot, axis=1)
    slot_of = chosen * capacity + place_in
    owner_ids = (
        jnp.zeros((experts_all * capacity,), jnp.int32)
        .at[slot_of]
        .set(jnp.arange(pair_count, dtype=jnp.int32) + 1)
    )
    owner_grid = owner_ids.reshape(sp_count, local_experts, capacity)
    part_slots = capacity // tp_count
    own_owners = lax.dynamic_slice_in_dim(owner_grid, tp_place * part_slots, part_slots, 2)
    source_row = jnp.maximum(own_owners - 1, 0) // top_count
    taken = normed[source_row.reshape(-1)].reshape(own_owners.shape + (model_width,))
    landed = lax.all_to_all(
        jnp.where((own_owners > 0)[..., None], taken, jnp.zeros((), jnp.bfloat16)),
        "sp",
        split_axis=0,
        concat_axis=0,
        tiled=True,
    )
    arrived = lax.all_gather(landed, "tp", axis=2, tiled=True)
    gate_part = jnp.einsum("sxcd,xdf->sxcf", arrived, exp_gate, preferred_element_type=jnp.float32)
    up_part = jnp.einsum("sxcd,xdf->sxcf", arrived, exp_up, preferred_element_type=jnp.float32)
    expert_hidden = (jax.nn.silu(gate_part) * up_part).astype(jnp.bfloat16)
    weight_rows = exp_down
    expert_sum = jnp.einsum(
        "sxcf,xfd->sxcd",
        lax.all_gather(expert_hidden, "tp", axis=3, tiled=True),
        weight_rows,
        preferred_element_type=jnp.float32,
    )
    expert_out = expert_sum.astype(jnp.bfloat16)
    returned = lax.all_to_all(expert_out, "sp", split_axis=0, concat_axis=0, tiled=True)
    flat_out = returned.reshape(experts_all * capacity, col_width)
    picked = flat_out[slot_of].astype(jnp.float32).reshape(tok_rows, top_count, col_width)
    routed = jnp.sum(picked * route_weights[:, :, None], axis=1)
    return (middle_cols.astype(jnp.float32) + shared + routed).astype(jnp.bfloat16)


ROW_CUTS = 2


def silu(value):
    return value / (1.0 + jnp.exp(-value))


def layer_kernel(
    levels,
    resid_hbm,
    a_val_hbm,
    a_gate_hbm,
    taps_hbm,
    conv_bias_hbm,
    ln_gain_hbm,
    ln_bias_hbm,
    w_out_hbm,
    ffn_gain_hbm,
    routes_ref,
    route_weights_ref,
    exp_gate_hbm,
    exp_up_hbm,
    exp_down_hbm,
    sh_gate_hbm,
    sh_up_hbm,
    sh_down_hbm,
    out_ref,
    resid_ref,
    a_val_ref,
    a_gate_ref,
    taps_ref,
    conv_bias_ref,
    ln_gain_ref,
    ln_bias_ref,
    w_out_ref,
    ffn_gain_ref,
    gate_ref,
    up_ref,
    down_ref,
    sh_gate_ref,
    sh_up_ref,
    sh_down_ref,
    halo_out,
    halo_in,
    padded_ref,
    conv_ref,
    stat_out,
    stat_in,
    give_out,
    give_in,
    keep_ref,
    chip_out,
    chip_in,
    rows_ref,
    normed_ref,
    hidden_ref,
    shared_ref,
    part_ref,
    back_ref,
    load_sem,
    halo_sem,
    stat_send,
    stat_recv,
    give_send,
    give_recv,
    chip_send,
    chip_recv,
    up_sem,
    low_sem,
    side_sem,
    core_sem,
    main_recv,
    core_recv,
    far_send,
    far_recv,
    near_send,
    near_recv,
    relay_send,
    relay_recv,
    shared_send,
    shared_recv,
    back_send,
    back_recv,
):
    count = 2 * levels
    me = lax.axis_index("sp")
    tp_place = lax.axis_index("tp")
    level, side = me // 2, me % 2
    row, core = tp_place // 2, tp_place % 2
    core_place = row * 2 + (1 - core)
    row_place = (1 - row) * 2 + core
    core_peer = {"tp": core_place}
    row_peer = {"tp": row_place}
    far_peer = {"tp": (1 - row) * 2 + (1 - core)}
    side_peer = {"sp": level * 2 + (1 - side)}
    mesh_ids = pl.DeviceIdType.MESH
    f32, bf16 = jnp.float32, jnp.bfloat16
    tok_rows, half_width = resid_ref.shape
    model_width = 2 * half_width
    col_width = out_ref.shape[1]
    span = taps_ref.shape[0]
    halo_rows = halo_in.shape[0]
    channels_all = 4 * a_val_ref.shape[1]
    part_hidden = gate_ref.shape[1]
    cut_rows = tok_rows // ROW_CUTS

    half_at = pl.ds(pl.multiple_of(core * half_width, half_width), half_width)
    pairs = [
        (a_val_hbm, a_val_ref),
        (a_gate_hbm, a_gate_ref),
        (taps_hbm, taps_ref),
        (conv_bias_hbm, conv_bias_ref),
        (ln_gain_hbm, ln_gain_ref),
        (ln_bias_hbm, ln_bias_ref),
        (w_out_hbm, w_out_ref),
        (resid_hbm.at[:, half_at], resid_ref),
        (ffn_gain_hbm, ffn_gain_ref),
        (exp_gate_hbm, gate_ref),
        (exp_up_hbm, up_ref),
        (sh_gate_hbm, sh_gate_ref),
        (sh_up_hbm, sh_up_ref),
        (exp_down_hbm, down_ref),
        (sh_down_hbm, sh_down_ref),
    ]
    loads = [
        pltpu.make_async_copy(src, dst, load_sem.at[at]) for at, (src, dst) in enumerate(pairs)
    ]
    for load in loads:
        load.start()

    barrier = pltpu.get_barrier_semaphore()
    others = [lax.rem(me + step, count) for step in range(1, count)]
    for other in others:
        pl.semaphore_signal(barrier, inc=1, device_id={"sp": other}, device_id_type=mesh_ids)
    for peer in (core_peer, row_peer, far_peer):
        pl.semaphore_signal(barrier, inc=1, device_id=peer, device_id_type=mesh_ids)

    def remote(src, dst, send, recv, where):
        return pltpu.make_async_remote_copy(
            src_ref=src, dst_ref=dst, send_sem=send, recv_sem=recv, device_id=where, device_id_type=mesh_ids
        )

    for load in loads[:4]:
        load.wait()
    gated = (a_val_ref[...].astype(f32) / (1.0 + jnp.exp(-a_gate_ref[...].astype(f32)))).astype(bf16)
    halo_out[...] = gated[tok_rows - halo_rows :]
    padded_ref[halo_rows:, :] = gated.astype(f32)
    taps = taps_ref[...].astype(f32)

    def convolve(first, size):
        total = jnp.broadcast_to(conv_bias_ref[...], (size, gated.shape[1]))
        for tap in range(span):
            at = first + tap + halo_rows - (span - 1)
            total = total + taps[tap : tap + 1] * padded_ref[at : at + size, :]
        conv_ref[first : first + size, :] = total

    pl.semaphore_wait(barrier, count + 2)
    halo = lambda where: remote(halo_out, halo_in, halo_sem.at[0], halo_sem.at[1], {"sp": where})

    @pl.when(me < count - 1)
    def _():
        halo(me + 1).start()

    convolve(halo_rows, tok_rows - halo_rows)

    @pl.when(me == 0)
    def _():
        padded_ref[:halo_rows, :] = jnp.zeros((halo_rows, gated.shape[1]), f32)

    @pl.when(me > 0)
    def _():
        halo(me).wait_recv()
        padded_ref[:halo_rows, :] = halo_in[...].astype(f32)

    convolve(0, halo_rows)

    conv_out = conv_ref[...]
    diagonal = lax.broadcasted_iota(jnp.int32, (tok_rows, tok_rows), 0) == lax.broadcasted_iota(
        jnp.int32, (tok_rows, tok_rows), 1
    )

    def lying(column):
        return jnp.sum(jnp.where(diagonal, column, 0.0), axis=0, keepdims=True)

    def standing(line):
        return jnp.sum(jnp.where(diagonal, line, 0.0), axis=1, keepdims=True)

    stat_out[0:1, :] = lying(jnp.sum(conv_out, axis=1, keepdims=True))
    stat_out[1:2, :] = lying(jnp.sum(conv_out * conv_out, axis=1, keepdims=True))
    stats = [
        remote(stat_out, stat_in.at[at], stat_send.at[at], stat_recv.at[at], peer)
        for at, peer in enumerate((core_peer, row_peer, far_peer))
    ]
    for copy in stats:
        copy.start()
    for load in loads[4:9]:
        load.wait()
    for copy in stats:
        copy.wait_recv()
    sums = (stat_out[...] + stat_in[0]) + (stat_in[1] + stat_in[2])
    channel_mean = standing(sums[0:1]) / channels_all
    channel_var = standing(sums[1:2]) / channels_all - channel_mean * channel_mean
    scaled = (conv_out - channel_mean) * lax.rsqrt(channel_var + LN_EPS) * ln_gain_ref[
        ...
    ] + ln_bias_ref[...]
    mixed = silu(scaled).astype(bf16)

    give_at = pl.ds(pl.multiple_of((1 - core) * half_width, half_width), half_width)
    give_out[...] = jnp.dot(mixed, w_out_ref[:, give_at], preferred_element_type=f32).astype(bf16)

    def cut(at):
        return pl.ds(at * cut_rows, cut_rows)

    gives = [
        remote(
            give_out.at[cut(at)], give_in.at[cut(at)], give_send.at[at], give_recv.at[at], core_peer
        )
        for at in range(ROW_CUTS)
    ]
    for copy in gives:
        copy.start()
    keep_ref[...] = jnp.dot(mixed, w_out_ref[:, half_at], preferred_element_type=f32)
    chips = [
        remote(
            chip_out.at[cut(at)], chip_in.at[cut(at)], chip_send.at[at], chip_recv.at[at], row_peer
        )
        for at in range(ROW_CUTS)
    ]
    for at in range(ROW_CUTS):
        gives[at].wait_recv()
        chip_sum = keep_ref[cut(at), :] + give_in[cut(at), :].astype(f32)
        keep_ref[cut(at), :] = chip_sum
        chip_out[cut(at), :] = chip_sum.astype(bf16)
        chips[at].start()

    def block(half, at, piece):
        return rows_ref.at[half, at, cut(piece)]

    def up_copy(origin, piece):
        at = origin * 2 + side
        sem = origin * ROW_CUTS + piece
        spot = block(core, at, piece)
        return remote(spot, spot, up_sem.at[sem], main_recv.at[at * ROW_CUTS + piece], {"sp": me + 2})

    def low_copy(origin, piece):
        at = origin * 2 + side
        sem = origin * ROW_CUTS + piece
        spot = block(core, at, piece)
        return remote(spot, spot, low_sem.at[sem], main_recv.at[at * ROW_CUTS + piece], {"sp": me - 2})

    def side_copy(origin, piece):
        at = origin * 2 + side
        sem = origin * ROW_CUTS + piece
        spot = block(core, at, piece)
        return remote(spot, spot, side_sem.at[sem], main_recv.at[at * ROW_CUTS + piece], side_peer)

    def core_copy(at, piece):
        sem = at * ROW_CUTS + piece
        spot = block(core, at, piece)
        return remote(spot, spot, core_sem.at[sem], core_recv.at[sem], core_peer)

    def landed(at, piece):
        spot = block(core, at, piece)
        sem = at * ROW_CUTS + piece
        remote(spot, spot, core_sem.at[sem], main_recv.at[sem], core_peer).wait_recv()

    def crossed(at, piece):
        spot = block(1 - core, at, piece)
        sem = at * ROW_CUTS + piece
        remote(spot, spot, core_sem.at[sem], core_recv.at[sem], core_peer).wait_recv()

    for at in range(ROW_CUTS):
        chips[at].wait_recv()
        total = keep_ref[cut(at), :] + chip_in[cut(at), :].astype(f32)
        rows_ref[core, me, cut(at), :] = (resid_ref[cut(at), :].astype(f32) + total).astype(bf16)
        core_copy(me, at).start()
        side_copy(level, at).start()

        @pl.when(level < levels - 1)
        def _():
            up_copy(level, at).start()

        @pl.when(level > 0)
        def _():
            low_copy(level, at).start()

    def normalise(at):
        low = rows_ref[0, at].astype(f32)
        high = rows_ref[1, at].astype(f32)
        power = jnp.sum(low * low, axis=1, keepdims=True) + jnp.sum(high * high, axis=1, keepdims=True)
        inverse = lax.rsqrt(power / model_width + RMS_EPS)
        normed_ref[:, :half_width] = (low * inverse * ffn_gain_ref[:, :half_width]).astype(bf16)
        normed_ref[:, half_width:] = (high * inverse * ffn_gain_ref[:, half_width:]).astype(bf16)

    def far_copy(at):
        spot = hidden_ref.at[tp_place, at]
        return remote(spot, spot, far_send.at[at], far_recv.at[at], row_peer)

    def near_copy(at):
        spot = hidden_ref.at[tp_place, at]
        return remote(spot, spot, near_send.at[at], near_recv.at[at], core_peer)

    def relay_copy(at):
        spot = hidden_ref.at[row_place, at]
        return remote(spot, spot, relay_send.at[at], relay_recv.at[at], core_peer)

    shared_far = remote(
        shared_ref.at[tp_place], shared_ref.at[tp_place], shared_send.at[0], shared_recv.at[0], row_peer
    )
    shared_near = remote(
        shared_ref.at[tp_place], shared_ref.at[tp_place], shared_send.at[1], shared_recv.at[1], core_peer
    )
    shared_relay = remote(
        shared_ref.at[row_place], shared_ref.at[row_place], shared_send.at[2], shared_recv.at[2], core_peer
    )

    def hide(at):
        for piece in range(ROW_CUTS):
            crossed(at, piece)
        normalise(at)
        step = 256
        for first in range(0, part_hidden, step):
            wide = slice(first, first + step)
            gate_part = jnp.dot(normed_ref[...], gate_ref[:, wide], preferred_element_type=f32)
            up_part = jnp.dot(normed_ref[...], up_ref[:, wide], preferred_element_type=f32)
            hidden_ref[tp_place, at, :, wide] = (silu(gate_part) * up_part).astype(bf16)
        far_copy(at).start()
        near_copy(at).start()

    def back_copy(at):
        return remote(part_ref.at[at], back_ref.at[me], back_send.at[at], back_recv.at[me], {"sp": at})

    def finish(at):
        far_copy(at).wait_recv()
        relay_copy(at).start()
        near_copy(at).wait_recv()
        relay_copy(at).wait_recv()
        total = jnp.zeros((tok_rows, col_width), f32)
        for place in range(4):
            total = total + jnp.dot(
                hidden_ref[place, at],
                down_ref[place * part_hidden : (place + 1) * part_hidden, :],
                preferred_element_type=f32,
            )
        result = total.astype(bf16)

        @pl.when(at == me)
        def _():
            back_ref[me] = result

        @pl.when(at != me)
        def _():
            part_ref[at] = result
            back_copy(at).start()

    turn = 1 - 2 * ((2 * level) // levels)

    def level_at(step):
        return lax.rem(level + turn * step + levels, levels)

    for load in loads[9:13]:
        load.wait()
    hide(me)
    shared_gate = jnp.dot(normed_ref[...], sh_gate_ref[...], preferred_element_type=f32)
    shared_up = jnp.dot(normed_ref[...], sh_up_ref[...], preferred_element_type=f32)
    shared_ref[tp_place] = (silu(shared_gate) * shared_up).astype(bf16)
    shared_far.start()
    shared_near.start()
    for load in loads[13:]:
        load.wait()

    def pass_on(step):
        below = level - step
        above = level + step

        @pl.when(below >= 0)
        def _():
            for piece in range(ROW_CUTS):
                landed(below * 2 + side, piece)
                core_copy(below * 2 + side, piece).start()
                side_copy(below, piece).start()

                @pl.when(level < levels - 1)
                def _():
                    up_copy(below, piece).start()

        @pl.when(above < levels)
        def _():
            for piece in range(ROW_CUTS):
                landed(above * 2 + side, piece)
                core_copy(above * 2 + side, piece).start()
                side_copy(above, piece).start()

                @pl.when(level > 0)
                def _():
                    low_copy(above, piece).start()

    def visit(step, before):
        near_level = level_at(step)
        own = near_level * 2 + side
        other = near_level * 2 + (1 - side)

        @pl.when(step > 0)
        def _():
            hide(own)
            finish(before)

        for piece in range(ROW_CUTS):
            landed(other, piece)
            core_copy(other, piece).start()

        @pl.when(step < levels - 1)
        def _():
            pass_on(step + 1)

        hide(other)
        finish(own)
        return other

    last = lax.fori_loop(0, levels, visit, me)
    finish(last)

    middle_cols = rows_ref[row, me, :, pl.ds(pl.multiple_of(core * col_width, col_width), col_width)]
    shared_far.wait_recv()
    shared_relay.start()
    shared_near.wait_recv()
    shared_relay.wait_recv()
    total = middle_cols.astype(f32)
    shared_width = shared_ref.shape[2]
    for place in range(4):
        total = total + jnp.dot(
            shared_ref[place],
            sh_down_ref[place * shared_width : (place + 1) * shared_width, :],
            preferred_element_type=f32,
        )
    routes = routes_ref[...]
    route_weights = route_weights_ref[...]
    for at in range(count):

        @pl.when(me != at)
        def _():
            remote(
                part_ref.at[at], back_ref.at[at], back_send.at[at], back_recv.at[at], core_peer
            ).wait_recv()

        weight = jnp.sum(jnp.where(routes == at, route_weights, 0.0), axis=1, keepdims=True)
        total = total + weight * back_ref[at].astype(f32)
    out_ref[...] = total.astype(bf16)

    @pl.when(me < count - 1)
    def _():
        halo(me + 1).wait_send()

    for copy in stats + gives + chips + [shared_far, shared_near, shared_relay]:
        copy.wait_send()

    @pl.loop(0, levels)
    def _(origin):
        for piece in range(ROW_CUTS):
            side_copy(origin, piece).wait_send()

            @pl.when((level < levels - 1) & (origin <= level))
            def _():
                up_copy(origin, piece).wait_send()

            @pl.when((level > 0) & (origin >= level))
            def _():
                low_copy(origin, piece).wait_send()

    @pl.loop(0, count)
    def _(at):
        for piece in range(ROW_CUTS):
            core_copy(at, piece).wait_send()
        far_copy(at).wait_send()
        near_copy(at).wait_send()
        relay_copy(at).wait_send()

        @pl.when(at != me)
        def _():
            back_copy(at).wait_send()


def body_dense(
    resid,
    a_val,
    a_gate,
    conv_kernel,
    conv_bias,
    ln_gain,
    ln_bias,
    w_out,
    ffn_gain,
    routes,
    route_weights,
    exp_gate,
    exp_up,
    exp_down,
    sh_gate,
    sh_up,
    sh_down,
):
    count = lax.axis_size("sp")
    levels = count // 2
    tok_rows, model_width = resid.shape
    half_width = model_width // 2
    channels = a_val.shape[1]
    part_hidden = exp_gate.shape[2]
    col_width = exp_down.shape[2]
    shared_width = sh_gate.shape[1]
    span = conv_kernel.shape[0]
    halo_rows = -(-(span - 1) // 16) * 16
    vmem = pl.BlockSpec(memory_space=pltpu.VMEM)
    hbm = pl.BlockSpec(memory_space=pltpu.HBM)
    f32, bf16 = jnp.float32, jnp.bfloat16
    dma = pltpu.SemaphoreType.DMA
    operands = (
        resid,
        a_val,
        a_gate,
        conv_kernel,
        conv_bias.reshape(1, -1),
        ln_gain.reshape(1, -1),
        ln_bias.reshape(1, -1),
        w_out,
        ffn_gain.reshape(1, -1),
        routes,
        route_weights,
        exp_gate[0],
        exp_up[0],
        exp_down[0],
        sh_gate,
        sh_up,
        sh_down,
    )
    pieces = count * ROW_CUTS
    return pl.pallas_call(
        functools.partial(layer_kernel, levels),
        out_shape=jax.ShapeDtypeStruct((tok_rows, col_width), bf16),
        in_specs=[hbm] * 9 + [vmem] * 2 + [hbm] * 6,
        out_specs=vmem,
        scratch_shapes=[
            pltpu.VMEM((tok_rows, half_width), bf16),
            pltpu.VMEM(a_val.shape, bf16),
            pltpu.VMEM(a_gate.shape, bf16),
            pltpu.VMEM(conv_kernel.shape, bf16),
            pltpu.VMEM((1, channels), f32),
            pltpu.VMEM((1, channels), f32),
            pltpu.VMEM((1, channels), f32),
            pltpu.VMEM(w_out.shape, bf16),
            pltpu.VMEM((1, model_width), f32),
            pltpu.VMEM(exp_gate.shape[1:], bf16),
            pltpu.VMEM(exp_up.shape[1:], bf16),
            pltpu.VMEM(exp_down.shape[1:], bf16),
            pltpu.VMEM(sh_gate.shape, bf16),
            pltpu.VMEM(sh_up.shape, bf16),
            pltpu.VMEM(sh_down.shape, bf16),
            pltpu.VMEM((halo_rows, channels), bf16),
            pltpu.VMEM((halo_rows, channels), bf16),
            pltpu.VMEM((halo_rows + tok_rows, channels), f32),
            pltpu.VMEM((tok_rows, channels), f32),
            pltpu.VMEM((2, tok_rows), f32),
            pltpu.VMEM((3, 2, tok_rows), f32),
            pltpu.VMEM((tok_rows, half_width), bf16),
            pltpu.VMEM((tok_rows, half_width), bf16),
            pltpu.VMEM((tok_rows, half_width), f32),
            pltpu.VMEM((tok_rows, half_width), bf16),
            pltpu.VMEM((tok_rows, half_width), bf16),
            pltpu.VMEM((2, count, tok_rows, half_width), bf16),
            pltpu.VMEM((tok_rows, model_width), bf16),
            pltpu.VMEM((4, count, tok_rows, part_hidden), bf16),
            pltpu.VMEM((4, tok_rows, shared_width), bf16),
            pltpu.VMEM((count, tok_rows, col_width), bf16),
            pltpu.VMEM((count, tok_rows, col_width), bf16),
            dma((15,)),
            dma((2,)),
            dma((3,)),
            dma((3,)),
            dma((ROW_CUTS,)),
            dma((ROW_CUTS,)),
            dma((ROW_CUTS,)),
            dma((ROW_CUTS,)),
            dma((levels * ROW_CUTS,)),
            dma((levels * ROW_CUTS,)),
            dma((levels * ROW_CUTS,)),
            dma((pieces,)),
            dma((pieces,)),
            dma((pieces,)),
            dma((count,)),
            dma((count,)),
            dma((count,)),
            dma((count,)),
            dma((count,)),
            dma((count,)),
            dma((3,)),
            dma((3,)),
            dma((count,)),
            dma((count,)),
        ],
        compiler_params=pltpu.CompilerParams(
            collective_id=0, has_side_effects=True, vmem_limit_bytes=56 * 1024 * 1024
        ),
    )(*operands)


def body(*args):
    tok_rows = args[0].shape[0]
    top_count = args[9].shape[1]
    local_experts = args[11].shape[0]
    experts_all = local_experts * lax.axis_size("sp")
    capacity = 2 * tok_rows * top_count // experts_all
    if (
        local_experts == 1
        and lax.axis_size("tp") == 4
        and lax.axis_size("sp") % 2 == 0
        and capacity >= tok_rows
    ):
        return body_dense(*args)
    return body_slots(*args)


def solution(mesh):
    in_specs = (
        P("sp", None),
        P("sp", "tp"),
        P("sp", "tp"),
        P(None, "tp"),
        P("tp"),
        P("tp"),
        P("tp"),
        P("tp", None),
        P(),
        P("sp", None),
        P("sp", None),
        P("sp", None, "tp"),
        P("sp", None, "tp"),
        P("sp", None, "tp"),
        P(None, "tp"),
        P(None, "tp"),
        P(None, "tp"),
    )
    out_specs = P("sp", "tp")
    return jax.shard_map(body, mesh=mesh, in_specs=in_specs, out_specs=out_specs, check_vma=False)
```

time: 161 us -> 91.3 us (0.57)
  waiting for transfers between devices: 45.3 us -> 0 us
  Pallas kernels: 51 us -> 86.7 us
  matrix products: 28.2 us -> 0 us
  blocking collectives: 11.8 us -> 0 us
  starting transfers between devices: 10.1 us -> 0 us
  other arithmetic: 5.25 us -> 0 us
  local copies, waits for them, and re-layouts: 8.6 us -> 4.39 us
    pallas_call x1, Pallas kernels: 51 us -> 86.7 us  [body_dense(): pl.pallas_call(functools.partial(layer_kernel, levels), out_shape=jax.Sha...]
    ppermute x5 -> x0, waiting for transfers between devices: 29.4 us -> none  [the longest x4 29.4 us: swapped(): return lax.ppermute(value, axis, [(i, i ^ bit) for i in range(size)])]
    dot_general x10 -> x0, matrix products: 28.2 us -> none  [the longest x1 6.63 us: body_dense(): gate_part = jnp.dot(rows, exp_gate[0], preferred_element_type=jnp.float32)]
    all_to_all x1 -> x0, waiting for transfers between devices: 16 us -> none  [body_dense(): lax.all_to_all(expert_sum.reshape(sp_count, tok_rows, col_width), 'sp', s...]
    ppermute x5 -> x0, starting transfers between devices: 6.36 us -> none  [the longest x1 4.88 us: shifted(): return lax.ppermute(value, axis, pairs)]
    psum x1 -> x0, blocking collectives: 6.33 us -> none  [body_dense(): lax.psum((jnp.sum(conv_out, axis=1), jnp.sum(conv_out * conv_out, axis=1)...]
    all_gather x1 -> x0, blocking collectives: 5.45 us -> none  [body_dense(): lax.all_gather(shared_hidden, 'tp', axis=1, tiled=True)]
    all_to_all x1 -> x0, starting transfers between devices: 3.69 us -> none  [body_dense(): lax.all_to_all(expert_sum.reshape(sp_count, tok_rows, col_width), 'sp', s...]
  transfers between devices with their start and end apart: 6 -> 0, of which waited for: 5 -> 0; matrix products, arithmetic and copies ran while one was open for 9% -> 0% of each run, Pallas kernels for 0% -> 0%
where the time goes in v1:
time: 91.3 us; the launch traced here: 91.1 us
  Pallas kernels  86.7 us (95%)
  local copies, waits for them, and re-layouts  4.39 us (5%)
    pallas_call x1, Pallas kernels, body_dense(): pl.pallas_call(functools.partial(layer_kernel, levels), out_shape=jax.Sha...  86.7 us
    unnamed x3, local copies, waits for them, and re-layouts  4.39 us

profile of v1, /device:TPU:0, one launch (start us, length us, event | category | flops | bytes accessed | tf_op | source)
XLA Modules:
  0.0 91.1 jit_solution(11011277497858713703)
XLA Ops:
  0.0 1.4 %copy.18.routes_ref = s32[128,4]{1,0:T(8,128)} copy(s32[128,4]{0,1:T(4,128)} %param.26) | data formatting | bytes 4096 | tf_op args[9]
  1.4 1.4 %copy.19.route_weights_ref = f32[128,4]{1,0:T(8,128)} copy(f32[128,4]{0,1:T(4,128)} %param.27) | data formatting | bytes 4096 | tf_op args[10]
  2.8 86.7 %shard_map.163 = bf16[128,512]{1,0:T(8,128)(2,1)} custom-call(bf16[128,2048]{1,0:T(8,128)(2,1)} %resid_hbm.1, bf16[128,256]{1,0:T(8,128)(2,1)} %a_val_hbm.1, bf16[128,256]{1,0:T(8,128)(2,1)} %a_gate_hbm.1, bf16[31,256]{1,0:T(8,128)(2,1)} %taps_hbm.1, f32[1,256]{1,0:T(1,128)} %bitcast.11, f32[1,256]{1,0:T(1,128)} %bitcast.12, f32[1,256]{1,0:T(1,128)} %bitcast.13, ...), custom_call_target="tpu_custom_call" | custom-call | tf_op jit(solution)/shard_map/pallas_call | solution.py:667
  89.6 1.6 %copy.21 = bf16[128,512]{1,0:T(8,128)(2,1)} copy(bf16[128,512]{1,0:T(8,128)(2,1)} %shard_map.163) | data formatting | bytes 262144

commit v2 on v1

--- a/solution.py
+++ b/solution.py
@@ -147,8 +147,8 @@
     ln_bias_hbm,
     w_out_hbm,
     ffn_gain_hbm,
-    routes_ref,
-    route_weights_ref,
+    routes_hbm,
+    route_weights_hbm,
     exp_gate_hbm,
     exp_up_hbm,
     exp_down_hbm,
@@ -165,6 +165,8 @@
     ln_bias_ref,
     w_out_ref,
     ffn_gain_ref,
+    routes_ref,
+    route_weights_ref,
     gate_ref,
     up_ref,
     down_ref,
@@ -188,6 +190,7 @@
     shared_ref,
     part_ref,
     back_ref,
+    sum_ref,
     load_sem,
     halo_sem,
     stat_send,
@@ -252,6 +255,8 @@
         (sh_up_hbm, sh_up_ref),
         (exp_down_hbm, down_ref),
         (sh_down_hbm, sh_down_ref),
+        (routes_hbm, routes_ref),
+        (route_weights_hbm, route_weights_ref),
     ]
     loads = [
         pltpu.make_async_copy(src, dst, load_sem.at[at]) for at, (src, dst) in enumerate(pairs)
@@ -260,11 +265,25 @@
         load.start()
 
     barrier = pltpu.get_barrier_semaphore()
-    others = [lax.rem(me + step, count) for step in range(1, count)]
-    for other in others:
-        pl.semaphore_signal(barrier, inc=1, device_id={"sp": other}, device_id_type=mesh_ids)
-    for peer in (core_peer, row_peer, far_peer):
+
+    def greet(peer):
         pl.semaphore_signal(barrier, inc=1, device_id=peer, device_id_type=mesh_ids)
+
+    across = ((side == 0) & (level > 0)) | ((side == 1) & (level < levels - 1))
+    for peer in (core_peer, row_peer, far_peer, side_peer):
+        greet(peer)
+
+    @pl.when(level > 0)
+    def _():
+        greet({"sp": me - 2})
+
+    @pl.when(level < levels - 1)
+    def _():
+        greet({"sp": me + 2})
+
+    @pl.when(across)
+    def _():
+        greet({"sp": me + 2 * side - 1})
 
     def remote(src, dst, send, recv, where):
         return pltpu.make_async_remote_copy(
@@ -285,7 +304,10 @@
             total = total + taps[tap : tap + 1] * padded_ref[at : at + size, :]
         conv_ref[first : first + size, :] = total
 
-    pl.semaphore_wait(barrier, count + 2)
+    has_below = (level + levels - 2) // (levels - 1)
+    has_above = (2 * levels - 3 - level) // (levels - 1)
+    has_across = has_below + side * (has_above - has_below)
+    pl.semaphore_wait(barrier, 4 + has_below + has_above + has_across)
     halo = lambda where: remote(halo_out, halo_in, halo_sem.at[0], halo_sem.at[1], {"sp": where})
 
     @pl.when(me < count - 1)
@@ -400,40 +422,43 @@
         sem = at * ROW_CUTS + piece
         remote(spot, spot, core_sem.at[sem], core_recv.at[sem], core_peer).wait_recv()
 
-    for at in range(ROW_CUTS):
-        chips[at].wait_recv()
-        total = keep_ref[cut(at), :] + chip_in[cut(at), :].astype(f32)
-        rows_ref[core, me, cut(at), :] = (resid_ref[cut(at), :].astype(f32) + total).astype(bf16)
-        core_copy(me, at).start()
-        side_copy(level, at).start()
+    def settle(piece):
+        chips[piece].wait_recv()
+        total = keep_ref[cut(piece), :] + chip_in[cut(piece), :].astype(f32)
+        rows_ref[core, me, cut(piece), :] = (resid_ref[cut(piece), :].astype(f32) + total).astype(bf16)
+        core_copy(me, piece).start()
+        side_copy(level, piece).start()
 
         @pl.when(level < levels - 1)
         def _():
-            up_copy(level, at).start()
+            up_copy(level, piece).start()
 
         @pl.when(level > 0)
         def _():
-            low_copy(level, at).start()
-
-    def normalise(at):
-        low = rows_ref[0, at].astype(f32)
-        high = rows_ref[1, at].astype(f32)
+            low_copy(level, piece).start()
+
+    def normalise(at, some):
+        low = rows_ref[0, at, some, :].astype(f32)
+        high = rows_ref[1, at, some, :].astype(f32)
         power = jnp.sum(low * low, axis=1, keepdims=True) + jnp.sum(high * high, axis=1, keepdims=True)
         inverse = lax.rsqrt(power / model_width + RMS_EPS)
-        normed_ref[:, :half_width] = (low * inverse * ffn_gain_ref[:, :half_width]).astype(bf16)
-        normed_ref[:, half_width:] = (high * inverse * ffn_gain_ref[:, half_width:]).astype(bf16)
-
-    def far_copy(at):
-        spot = hidden_ref.at[tp_place, at]
-        return remote(spot, spot, far_send.at[at], far_recv.at[at], row_peer)
-
-    def near_copy(at):
-        spot = hidden_ref.at[tp_place, at]
-        return remote(spot, spot, near_send.at[at], near_recv.at[at], core_peer)
-
-    def relay_copy(at):
-        spot = hidden_ref.at[row_place, at]
-        return remote(spot, spot, relay_send.at[at], relay_recv.at[at], core_peer)
+        normed_ref[some, :half_width] = (low * inverse * ffn_gain_ref[:, :half_width]).astype(bf16)
+        normed_ref[some, half_width:] = (high * inverse * ffn_gain_ref[:, half_width:]).astype(bf16)
+
+    def far_copy(at, piece):
+        spot = hidden_ref.at[tp_place, at, cut(piece)]
+        sem = at * ROW_CUTS + piece
+        return remote(spot, spot, far_send.at[sem], far_recv.at[sem], row_peer)
+
+    def near_copy(at, piece):
+        spot = hidden_ref.at[tp_place, at, cut(piece)]
+        sem = at * ROW_CUTS + piece
+        return remote(spot, spot, near_send.at[sem], near_recv.at[sem], core_peer)
+
+    def relay_copy(at, piece):
+        spot = hidden_ref.at[row_place, at, cut(piece)]
+        sem = at * ROW_CUTS + piece
+        return remote(spot, spot, relay_send.at[sem], relay_recv.at[sem], core_peer)
 
     shared_far = remote(
         shared_ref.at[tp_place], shared_ref.at[tp_place], shared_send.at[0], shared_recv.at[0], row_peer
@@ -445,111 +470,149 @@
         shared_ref.at[row_place], shared_ref.at[row_place], shared_send.at[2], shared_recv.at[2], core_peer
     )
 
-    def hide(at):
-        for piece in range(ROW_CUTS):
+    every = range(ROW_CUTS)
+
+    def hide(at, pieces):
+        some = pl.ds(pieces[0] * cut_rows, len(pieces) * cut_rows)
+        for piece in pieces:
             crossed(at, piece)
-        normalise(at)
+        normalise(at, some)
+        hide_rows(at, pieces)
+
+    def hide_rows(at, pieces):
+        some = pl.ds(pieces[0] * cut_rows, len(pieces) * cut_rows)
         step = 256
         for first in range(0, part_hidden, step):
             wide = slice(first, first + step)
-            gate_part = jnp.dot(normed_ref[...], gate_ref[:, wide], preferred_element_type=f32)
-            up_part = jnp.dot(normed_ref[...], up_ref[:, wide], preferred_element_type=f32)
-            hidden_ref[tp_place, at, :, wide] = (silu(gate_part) * up_part).astype(bf16)
-        far_copy(at).start()
-        near_copy(at).start()
+            gate_part = jnp.dot(normed_ref[some, :], gate_ref[:, wide], preferred_element_type=f32)
+            up_part = jnp.dot(normed_ref[some, :], up_ref[:, wide], preferred_element_type=f32)
+            hidden_ref[tp_place, at, some, wide] = (silu(gate_part) * up_part).astype(bf16)
+        for piece in pieces:
+            far_copy(at, piece).start()
+        for piece in pieces:
+            near_copy(at, piece).start()
+
+    def down_part(at, some, place):
+        return jnp.dot(
+            hidden_ref[place, at, some, :],
+            down_ref[pl.ds(pl.multiple_of(place * part_hidden, part_hidden), part_hidden), :],
+            preferred_element_type=f32,
+        )
 
     def back_copy(at):
         return remote(part_ref.at[at], back_ref.at[me], back_send.at[at], back_recv.at[me], {"sp": at})
 
+    def relay(at, piece):
+        far_copy(at, piece).wait_recv()
+        relay_copy(at, piece).start()
+
     def finish(at):
-        far_copy(at).wait_recv()
-        relay_copy(at).start()
-        near_copy(at).wait_recv()
-        relay_copy(at).wait_recv()
-        total = jnp.zeros((tok_rows, col_width), f32)
-        for place in range(4):
-            total = total + jnp.dot(
-                hidden_ref[place, at],
-                down_ref[place * part_hidden : (place + 1) * part_hidden, :],
-                preferred_element_type=f32,
-            )
-        result = total.astype(bf16)
-
-        @pl.when(at == me)
+        for piece in every:
+            relay(at, piece)
+        for piece in every:
+            near_copy(at, piece).wait_recv()
+        for piece in every:
+            relay_copy(at, piece).wait_recv()
+        some = pl.ds(0, tok_rows)
+        total = (down_part(at, some, 0) + down_part(at, some, 1)) + (
+            down_part(at, some, 2) + down_part(at, some, 3)
+        )
+        part_ref[at] = total.astype(bf16)
+        back_copy(at).start()
+
+    def pass_on(step, piece):
+        below = level - step
+        above = level + step
+
+        @pl.when(below >= 0)
         def _():
-            back_ref[me] = result
-
-        @pl.when(at != me)
+            landed(below * 2 + side, piece)
+
+            @pl.when(level < levels - 1)
+            def _():
+                up_copy(below, piece).start()
+
+            side_copy(below, piece).start()
+            core_copy(below * 2 + side, piece).start()
+
+        @pl.when(above < levels)
         def _():
-            part_ref[at] = result
-            back_copy(at).start()
-
-    turn = 1 - 2 * ((2 * level) // levels)
-
-    def level_at(step):
-        return lax.rem(level + turn * step + levels, levels)
-
+            landed(above * 2 + side, piece)
+
+            @pl.when(level > 0)
+            def _():
+                low_copy(above, piece).start()
+
+            side_copy(above, piece).start()
+            core_copy(above * 2 + side, piece).start()
+
+    def from_side(at):
+        for piece in every:
+            landed(at, piece)
+            core_copy(at, piece).start()
+
+    upper = (2 * level) // levels
+    inner = level + upper * (levels - 1 - 2 * level)
+
+    def visited(outer_way, inner_way):
+        mirrored = outer_way[0] + inner * (inner_way[0] - outer_way[0])
+        other = outer_way[1] + inner * (inner_way[1] - outer_way[1])
+        at_level = mirrored + upper * (levels - 1 - 2 * mirrored)
+        return at_level * 2 + lax.rem(side + other, 2), other
+
+    outer_order = ((0, 1), (1, 0), (2, 0), (3, 0), (2, 1), (3, 1), (1, 1))
+    inner_order = ((0, 0), (2, 0), (3, 0), (2, 1), (0, 1), (3, 1), (1, 1))
+    visits = [visited(*ways) for ways in zip(outer_order, inner_order)]
+
+    settle(0)
     for load in loads[9:13]:
         load.wait()
-    hide(me)
+    hide(me, (0,))
+    settle(1)
+    first = visits[0][0]
+    beside = level * 2 + (1 - side)
+    for piece in every:
+        landed(beside, piece)
+        core_copy(beside, piece).start()
+        pass_on(1, piece)
+        hide(first, (piece,))
+    for load in loads[13:]:
+        load.wait()
+    hide(visits[1][0], every)
+    for piece in every:
+        pass_on(2, piece)
+    relay(me, 0)
+    finish(first)
+
+    crossed(me, 1)
+    whole = pl.ds(0, tok_rows)
+    normalise(me, whole)
     shared_gate = jnp.dot(normed_ref[...], sh_gate_ref[...], preferred_element_type=f32)
     shared_up = jnp.dot(normed_ref[...], sh_up_ref[...], preferred_element_type=f32)
     shared_ref[tp_place] = (silu(shared_gate) * shared_up).astype(bf16)
-    shared_far.start()
-    shared_near.start()
-    for load in loads[13:]:
-        load.wait()
-
-    def pass_on(step):
-        below = level - step
-        above = level + step
-
-        @pl.when(below >= 0)
-        def _():
-            for piece in range(ROW_CUTS):
-                landed(below * 2 + side, piece)
-                core_copy(below * 2 + side, piece).start()
-                side_copy(below, piece).start()
-
-                @pl.when(level < levels - 1)
+
+    for turn in range(2, len(visits)):
+        at, other = visits[turn]
+        hide(at, every)
+        if turn == 2:
+            for piece in every:
+                pass_on(3, piece)
+            shared_far.start()
+            shared_near.start()
+        if turn + 1 < len(visits):
+            after, after_other = visits[turn + 1]
+
+            @pl.when(after_other == 1)
+            def _():
+                @pl.when(after != beside)
                 def _():
-                    up_copy(below, piece).start()
-
-        @pl.when(above < levels)
-        def _():
-            for piece in range(ROW_CUTS):
-                landed(above * 2 + side, piece)
-                core_copy(above * 2 + side, piece).start()
-                side_copy(above, piece).start()
-
-                @pl.when(level > 0)
-                def _():
-                    low_copy(above, piece).start()
-
-    def visit(step, before):
-        near_level = level_at(step)
-        own = near_level * 2 + side
-        other = near_level * 2 + (1 - side)
-
-        @pl.when(step > 0)
-        def _():
-            hide(own)
-            finish(before)
-
-        for piece in range(ROW_CUTS):
-            landed(other, piece)
-            core_copy(other, piece).start()
-
-        @pl.when(step < levels - 1)
-        def _():
-            pass_on(step + 1)
-
-        hide(other)
-        finish(own)
-        return other
-
-    last = lax.fori_loop(0, levels, visit, me)
-    finish(last)
+                    from_side(after)
+
+        finish(visits[turn - 1][0])
+
+    normalise(me, cut(1))
+    hide_rows(me, (1,))
+    finish(visits[-1][0])
 
     middle_cols = rows_ref[row, me, :, pl.ds(pl.multiple_of(core * col_width, col_width), col_width)]
     shared_far.wait_recv()
@@ -564,17 +627,28 @@
             sh_down_ref[place * shared_width : (place + 1) * shared_width, :],
             preferred_element_type=f32,
         )
+    sum_ref[...] = total
+
+    for piece in every:
+        near_copy(me, piece).wait_recv()
+    relay_copy(me, 0).wait_recv()
+    own_part = down_part(me, whole, tp_place) + down_part(me, whole, core_place)
+    relay(me, 1)
+    own_part = own_part + down_part(me, whole, row_place)
+    relay_copy(me, 1).wait_recv()
+    own_part = own_part + down_part(me, whole, (1 - row) * 2 + (1 - core))
+    part_ref[me] = own_part.astype(bf16)
+    total = sum_ref[...]
     routes = routes_ref[...]
     route_weights = route_weights_ref[...]
-    for at in range(count):
-
-        @pl.when(me != at)
-        def _():
-            remote(
-                part_ref.at[at], back_ref.at[at], back_send.at[at], back_recv.at[at], core_peer
-            ).wait_recv()
-
-        weight = jnp.sum(jnp.where(routes == at, route_weights, 0.0), axis=1, keepdims=True)
+    own_weight = standing(jnp.sum(jnp.where(routes == me, route_weights, 0.0), axis=0, keepdims=True))
+    total = total + own_weight * part_ref[me].astype(f32)
+    for step in range(1, count):
+        at = lax.rem(me + step, count)
+        remote(
+            part_ref.at[at], back_ref.at[at], back_send.at[at], back_recv.at[at], core_peer
+        ).wait_recv()
+        weight = standing(jnp.sum(jnp.where(routes == at, route_weights, 0.0), axis=0, keepdims=True))
         total = total + weight * back_ref[at].astype(f32)
     out_ref[...] = total.astype(bf16)
 
@@ -600,11 +674,11 @@
 
     @pl.loop(0, count)
     def _(at):
-        for piece in range(ROW_CUTS):
+        for piece in every:
             core_copy(at, piece).wait_send()
-        far_copy(at).wait_send()
-        near_copy(at).wait_send()
-        relay_copy(at).wait_send()
+            far_copy(at, piece).wait_send()
+            near_copy(at, piece).wait_send()
+            relay_copy(at, piece).wait_send()
 
         @pl.when(at != me)
         def _():
@@ -638,6 +712,7 @@
     part_hidden = exp_gate.shape[2]
     col_width = exp_down.shape[2]
     shared_width = sh_gate.shape[1]
+    top_count = routes.shape[1]
     span = conv_kernel.shape[0]
     halo_rows = -(-(span - 1) // 16) * 16
     vmem = pl.BlockSpec(memory_space=pltpu.VMEM)
@@ -654,8 +729,8 @@
         ln_bias.reshape(1, -1),
         w_out,
         ffn_gain.reshape(1, -1),
-        routes,
-        route_weights,
+        routes.T,
+        route_weights.T,
         exp_gate[0],
         exp_up[0],
         exp_down[0],
@@ -667,7 +742,7 @@
     return pl.pallas_call(
         functools.partial(layer_kernel, levels),
         out_shape=jax.ShapeDtypeStruct((tok_rows, col_width), bf16),
-        in_specs=[hbm] * 9 + [vmem] * 2 + [hbm] * 6,
+        in_specs=[hbm] * len(operands),
         out_specs=vmem,
         scratch_shapes=[
             pltpu.VMEM((tok_rows, half_width), bf16),
@@ -679,6 +754,8 @@
             pltpu.VMEM((1, channels), f32),
             pltpu.VMEM(w_out.shape, bf16),
             pltpu.VMEM((1, model_width), f32),
+            pltpu.VMEM((top_count, tok_rows), jnp.int32),
+            pltpu.VMEM((top_count, tok_rows), f32),
             pltpu.VMEM(exp_gate.shape[1:], bf16),
             pltpu.VMEM(exp_up.shape[1:], bf16),
             pltpu.VMEM(exp_down.shape[1:], bf16),
@@ -702,7 +779,8 @@
             pltpu.VMEM((4, tok_rows, shared_width), bf16),
             pltpu.VMEM((count, tok_rows, col_width), bf16),
             pltpu.VMEM((count, tok_rows, col_width), bf16),
-            dma((15,)),
+            pltpu.VMEM((tok_rows, col_width), f32),
+            dma((17,)),
             dma((2,)),
             dma((3,)),
             dma((3,)),
@@ -716,12 +794,12 @@
             dma((pieces,)),
             dma((pieces,)),
             dma((pieces,)),
-            dma((count,)),
-            dma((count,)),
-            dma((count,)),
-            dma((count,)),
-            dma((count,)),
-            dma((count,)),
+            dma((pieces,)),
+            dma((pieces,)),
+            dma((pieces,)),
+            dma((pieces,)),
+            dma((pieces,)),
+            dma((pieces,)),
             dma((3,)),
             dma((3,)),
             dma((count,)),
@@ -742,7 +820,7 @@
     if (
         local_experts == 1
         and lax.axis_size("tp") == 4
-        and lax.axis_size("sp") % 2 == 0
+        and lax.axis_size("sp") == 8
         and capacity >= tok_rows
     ):
         return body_dense(*args)

time: 91.3 us -> 80.6 us (0.88)
  the two profiles are of different devices: /device:TPU:0 before, /device:TPU:17 now
where the time goes in v2:
time: 80.6 us; the launch traced here: 80.5 us
  Pallas kernels  78.9 us (98%)
  local copies, waits for them, and re-layouts  1.57 us (2%)
    pallas_call x1, Pallas kernels, body_dense(): pl.pallas_call(functools.partial(layer_kernel, levels), out_shape=jax.Sha...  78.9 us

profile of v2, /device:TPU:17, one launch (start us, length us, event | category | flops | bytes accessed | tf_op | source)
XLA Modules:
  0.0 80.5 jit_solution(1117056461777660212)
XLA Ops:
  0.0 78.9 %shard_map.163 = bf16[128,512]{1,0:T(8,128)(2,1)} custom-call(bf16[128,2048]{1,0:T(8,128)(2,1)} %resid_hbm.1, bf16[128,256]{1,0:T(8,128)(2,1)} %a_val_hbm.1, bf16[128,256]{1,0:T(8,128)(2,1)} %a_gate_hbm.1, bf16[31,256]{1,0:T(8,128)(2,1)} %taps_hbm.1, f32[1,256]{1,0:T(1,128)} %bitcast.15, f32[1,256]{1,0:T(1,128)} %bitcast.16, f32[1,256]{1,0:T(1,128)} %bitcast.17, ...), custom_call_target="tpu_custom_call" | custom-call | tf_op jit(solution)/shard_map/pallas_call | solution.py:742
  78.9 1.6 %copy.19 = bf16[128,512]{1,0:T(8,128)(2,1)} copy(bf16[128,512]{1,0:T(8,128)(2,1)} %shard_map.163) | data formatting | bytes 262144

commit v3 on v2

--- a/solution.py
+++ b/solution.py
@@ -179,8 +179,9 @@
     conv_ref,
     stat_out,
     stat_in,
-    give_out,
-    give_in,
+    mix_out,
+    mix_in,
+    w_in,
     keep_ref,
     chip_out,
     chip_in,
@@ -195,8 +196,7 @@
     halo_sem,
     stat_send,
     stat_recv,
-    give_send,
-    give_recv,
+    mix_sem,
     chip_send,
     chip_recv,
     up_sem,
@@ -246,7 +246,7 @@
         (conv_bias_hbm, conv_bias_ref),
         (ln_gain_hbm, ln_gain_ref),
         (ln_bias_hbm, ln_bias_ref),
-        (w_out_hbm, w_out_ref),
+        (w_out_hbm.at[:, half_at], w_out_ref),
         (resid_hbm.at[:, half_at], resid_ref),
         (ffn_gain_hbm, ffn_gain_ref),
         (exp_gate_hbm, gate_ref),
@@ -308,12 +308,15 @@
     has_above = (2 * levels - 3 - level) // (levels - 1)
     has_across = has_below + side * (has_above - has_below)
     pl.semaphore_wait(barrier, 4 + has_below + has_above + has_across)
+    give_at = pl.ds(pl.multiple_of((1 - core) * half_width, half_width), half_width)
+    w_swap = remote(w_out_hbm.at[:, give_at], w_in, mix_sem.at[2], mix_sem.at[3], core_peer)
     halo = lambda where: remote(halo_out, halo_in, halo_sem.at[0], halo_sem.at[1], {"sp": where})
 
     @pl.when(me < count - 1)
     def _():
         halo(me + 1).start()
 
+    w_swap.start()
     convolve(halo_rows, tok_rows - halo_rows)
 
     @pl.when(me == 0)
@@ -356,32 +359,26 @@
     scaled = (conv_out - channel_mean) * lax.rsqrt(channel_var + LN_EPS) * ln_gain_ref[
         ...
     ] + ln_bias_ref[...]
-    mixed = silu(scaled).astype(bf16)
-
-    give_at = pl.ds(pl.multiple_of((1 - core) * half_width, half_width), half_width)
-    give_out[...] = jnp.dot(mixed, w_out_ref[:, give_at], preferred_element_type=f32).astype(bf16)
+    mix_out[...] = silu(scaled).astype(bf16)
 
     def cut(at):
         return pl.ds(at * cut_rows, cut_rows)
 
-    gives = [
-        remote(
-            give_out.at[cut(at)], give_in.at[cut(at)], give_send.at[at], give_recv.at[at], core_peer
-        )
-        for at in range(ROW_CUTS)
-    ]
-    for copy in gives:
-        copy.start()
-    keep_ref[...] = jnp.dot(mixed, w_out_ref[:, half_at], preferred_element_type=f32)
+    mix = remote(mix_out, mix_in, mix_sem.at[0], mix_sem.at[1], core_peer)
+    mix.start()
+    keep_ref[...] = jnp.dot(mix_out[...], w_out_ref[...], preferred_element_type=f32)
+    w_swap.wait_recv()
     chips = [
         remote(
             chip_out.at[cut(at)], chip_in.at[cut(at)], chip_send.at[at], chip_recv.at[at], row_peer
         )
         for at in range(ROW_CUTS)
     ]
+    mix.wait_recv()
     for at in range(ROW_CUTS):
-        gives[at].wait_recv()
-        chip_sum = keep_ref[cut(at), :] + give_in[cut(at), :].astype(f32)
+        chip_sum = keep_ref[cut(at), :] + jnp.dot(
+            mix_in[cut(at), :], w_in[...], preferred_element_type=f32
+        )
         keep_ref[cut(at), :] = chip_sum
         chip_out[cut(at), :] = chip_sum.astype(bf16)
         chips[at].start()
@@ -499,26 +496,33 @@
             preferred_element_type=f32,
         )
 
-    def back_copy(at):
-        return remote(part_ref.at[at], back_ref.at[me], back_send.at[at], back_recv.at[me], {"sp": at})
+    def back_copy(at, piece):
+        return remote(
+            part_ref.at[at, cut(piece)],
+            back_ref.at[me, cut(piece)],
+            back_send.at[at * ROW_CUTS + piece],
+            back_recv.at[me * ROW_CUTS + piece],
+            {"sp": at},
+        )
 
     def relay(at, piece):
         far_copy(at, piece).wait_recv()
         relay_copy(at, piece).start()
 
-    def finish(at):
-        for piece in every:
+    def finish(at, pieces):
+        for piece in pieces:
             relay(at, piece)
-        for piece in every:
+        for piece in pieces:
             near_copy(at, piece).wait_recv()
-        for piece in every:
+        for piece in pieces:
             relay_copy(at, piece).wait_recv()
-        some = pl.ds(0, tok_rows)
+        some = pl.ds(pieces[0] * cut_rows, len(pieces) * cut_rows)
         total = (down_part(at, some, 0) + down_part(at, some, 1)) + (
             down_part(at, some, 2) + down_part(at, some, 3)
         )
-        part_ref[at] = total.astype(bf16)
-        back_copy(at).start()
+        part_ref[at, some, :] = total.astype(bf16)
+        for piece in pieces:
+            back_copy(at, piece).start()
 
     def pass_on(step, piece):
         below = level - step
@@ -582,38 +586,37 @@
     for piece in every:
         pass_on(2, piece)
     relay(me, 0)
-    finish(first)
-
-    crossed(me, 1)
     whole = pl.ds(0, tok_rows)
-    normalise(me, whole)
-    shared_gate = jnp.dot(normed_ref[...], sh_gate_ref[...], preferred_element_type=f32)
-    shared_up = jnp.dot(normed_ref[...], sh_up_ref[...], preferred_element_type=f32)
-    shared_ref[tp_place] = (silu(shared_gate) * shared_up).astype(bf16)
+
+    def fetch(turn):
+        at, other = visits[turn]
+
+        @pl.when(other == 1)
+        def _():
+            @pl.when(at != beside)
+            def _():
+                from_side(at)
 
     for turn in range(2, len(visits)):
-        at, other = visits[turn]
+        at = visits[turn][0]
         hide(at, every)
+        if turn + 1 < len(visits):
+            fetch(turn + 1)
+        finish(visits[turn - 2][0], every)
         if turn == 2:
             for piece in every:
                 pass_on(3, piece)
+        if turn == 4:
+            crossed(me, 1)
+            normalise(me, whole)
+            shared_gate = jnp.dot(normed_ref[...], sh_gate_ref[...], preferred_element_type=f32)
+            shared_up = jnp.dot(normed_ref[...], sh_up_ref[...], preferred_element_type=f32)
+            shared_ref[tp_place] = (silu(shared_gate) * shared_up).astype(bf16)
             shared_far.start()
             shared_near.start()
-        if turn + 1 < len(visits):
-            after, after_other = visits[turn + 1]
-
-            @pl.when(after_other == 1)
-            def _():
-                @pl.when(after != beside)
-                def _():
-                    from_side(after)
-
-        finish(visits[turn - 1][0])
 
     normalise(me, cut(1))
     hide_rows(me, (1,))
-    finish(visits[-1][0])
-
     middle_cols = rows_ref[row, me, :, pl.ds(pl.multiple_of(core * col_width, col_width), col_width)]
     shared_far.wait_recv()
     shared_relay.start()
@@ -628,6 +631,9 @@
             preferred_element_type=f32,
         )
     sum_ref[...] = total
+    finish(visits[-2][0], every)
+    for piece in every:
+        finish(visits[-1][0], (piece,))
 
     for piece in every:
         near_copy(me, piece).wait_recv()
@@ -645,9 +651,14 @@
     total = total + own_weight * part_ref[me].astype(f32)
     for step in range(1, count):
         at = lax.rem(me + step, count)
-        remote(
-            part_ref.at[at], back_ref.at[at], back_send.at[at], back_recv.at[at], core_peer
-        ).wait_recv()
+        for piece in every:
+            remote(
+                part_ref.at[at, cut(piece)],
+                back_ref.at[at, cut(piece)],
+                back_send.at[at * ROW_CUTS + piece],
+                back_recv.at[at * ROW_CUTS + piece],
+                core_peer,
+            ).wait_recv()
         weight = standing(jnp.sum(jnp.where(routes == at, route_weights, 0.0), axis=0, keepdims=True))
         total = total + weight * back_ref[at].astype(f32)
     out_ref[...] = total.astype(bf16)
@@ -656,7 +667,7 @@
     def _():
         halo(me + 1).wait_send()
 
-    for copy in stats + gives + chips + [shared_far, shared_near, shared_relay]:
+    for copy in stats + chips + [w_swap, mix, shared_far, shared_near, shared_relay]:
         copy.wait_send()
 
     @pl.loop(0, levels)
@@ -682,7 +693,8 @@
 
         @pl.when(at != me)
         def _():
-            back_copy(at).wait_send()
+            for piece in every:
+                back_copy(at, piece).wait_send()
 
 
 def body_dense(
@@ -752,7 +764,7 @@
             pltpu.VMEM((1, channels), f32),
             pltpu.VMEM((1, channels), f32),
             pltpu.VMEM((1, channels), f32),
-            pltpu.VMEM(w_out.shape, bf16),
+            pltpu.VMEM((channels, half_width), bf16),
             pltpu.VMEM((1, model_width), f32),
             pltpu.VMEM((top_count, tok_rows), jnp.int32),
             pltpu.VMEM((top_count, tok_rows), f32),
@@ -768,8 +780,9 @@
             pltpu.VMEM((tok_rows, channels), f32),
             pltpu.VMEM((2, tok_rows), f32),
             pltpu.VMEM((3, 2, tok_rows), f32),
-            pltpu.VMEM((tok_rows, half_width), bf16),
-            pltpu.VMEM((tok_rows, half_width), bf16),
+            pltpu.VMEM((tok_rows, channels), bf16),
+            pltpu.VMEM((tok_rows, channels), bf16),
+            pltpu.VMEM((channels, half_width), bf16),
             pltpu.VMEM((tok_rows, half_width), f32),
             pltpu.VMEM((tok_rows, half_width), bf16),
             pltpu.VMEM((tok_rows, half_width), bf16),
@@ -784,8 +797,7 @@
             dma((2,)),
             dma((3,)),
             dma((3,)),
-            dma((ROW_CUTS,)),
-            dma((ROW_CUTS,)),
+            dma((4,)),
             dma((ROW_CUTS,)),
             dma((ROW_CUTS,)),
             dma((levels * ROW_CUTS,)),
@@ -802,8 +814,8 @@
             dma((pieces,)),
             dma((3,)),
             dma((3,)),
-            dma((count,)),
-            dma((count,)),
+            dma((pieces,)),
+            dma((pieces,)),
         ],
         compiler_params=pltpu.CompilerParams(
             collective_id=0, has_side_effects=True, vmem_limit_bytes=56 * 1024 * 1024

time: 80.6 us -> 77.8 us (0.965)
  the two profiles are of different devices: /device:TPU:17 before, /device:TPU:0 now
where the time goes in v3:
time: 77.8 us; the launch traced here: 77.6 us
  Pallas kernels  76 us (98%)
  local copies, waits for them, and re-layouts  1.57 us (2%)
    pallas_call x1, Pallas kernels, body_dense(): pl.pallas_call(functools.partial(layer_kernel, levels), out_shape=jax.Sha...  76 us
    unnamed x1, local copies, waits for them, and re-layouts  1.57 us

profile of v3, /device:TPU:0, one launch (start us, length us, event | category | flops | bytes accessed | tf_op | source)
XLA Modules:
  0.0 77.6 jit_solution(13819507261975136097)
XLA Ops:
  0.0 76.0 %shard_map.163 = bf16[128,512]{1,0:T(8,128)(2,1)} custom-call(bf16[128,2048]{1,0:T(8,128)(2,1)} %resid_hbm.1, bf16[128,256]{1,0:T(8,128)(2,1)} %a_val_hbm.1, bf16[128,256]{1,0:T(8,128)(2,1)} %a_gate_hbm.1, bf16[31,256]{1,0:T(8,128)(2,1)} %taps_hbm.1, f32[1,256]{1,0:T(1,128)} %bitcast.15, f32[1,256]{1,0:T(1,128)} %bitcast.16, f32[1,256]{1,0:T(1,128)} %bitcast.17, ...), custom_call_target="tpu_custom_call" | custom-call | tf_op jit(solution)/shard_map/pallas_call | solution.py:754
  76.0 1.6 %copy.19 = bf16[128,512]{1,0:T(8,128)(2,1)} copy(bf16[128,512]{1,0:T(8,128)(2,1)} %shard_map.163) | data formatting | bytes 262144

commit v4 on v3

--- a/solution.py
+++ b/solution.py
@@ -129,7 +129,7 @@
     return (middle_cols.astype(jnp.float32) + shared + routed).astype(jnp.bfloat16)
 
 
-ROW_CUTS = 2
+ROW_CUTS = 4
 
 
 def silu(value):
@@ -304,20 +304,55 @@
             total = total + taps[tap : tap + 1] * padded_ref[at : at + size, :]
         conv_ref[first : first + size, :] = total
 
+    diagonal = lax.broadcasted_iota(jnp.int32, (tok_rows, tok_rows), 0) == lax.broadcasted_iota(
+        jnp.int32, (tok_rows, tok_rows), 1
+    )
+
+    def lying(column, first):
+        mask = diagonal[first : first + column.shape[0]]
+        return jnp.sum(jnp.where(mask, column, 0.0), axis=0, keepdims=True)
+
+    def standing(line, first, size):
+        mask = diagonal[first : first + size]
+        return jnp.sum(jnp.where(mask, line, 0.0), axis=1, keepdims=True)
+
+    def measure(first, size, part):
+        rows = conv_ref[first : first + size, :]
+        stat_out[part, 0:1, :] = lying(jnp.sum(rows, axis=1, keepdims=True), first)
+        stat_out[part, 1:2, :] = lying(jnp.sum(rows * rows, axis=1, keepdims=True), first)
+
+    stats = [
+        [
+            remote(
+                stat_out.at[part],
+                stat_in.at[part, at],
+                stat_send.at[part * 3 + at],
+                stat_recv.at[part * 3 + at],
+                peer,
+            )
+            for at, peer in enumerate((core_peer, row_peer, far_peer))
+        ]
+        for part in range(2)
+    ]
+    rest = tok_rows - halo_rows
+    convolve(halo_rows, rest)
+    measure(halo_rows, rest, 0)
+
     has_below = (level + levels - 2) // (levels - 1)
     has_above = (2 * levels - 3 - level) // (levels - 1)
     has_across = has_below + side * (has_above - has_below)
     pl.semaphore_wait(barrier, 4 + has_below + has_above + has_across)
     give_at = pl.ds(pl.multiple_of((1 - core) * half_width, half_width), half_width)
-    w_swap = remote(w_out_hbm.at[:, give_at], w_in, mix_sem.at[2], mix_sem.at[3], core_peer)
+    w_swap = remote(w_out_hbm.at[:, give_at], w_in, mix_sem.at[0], mix_sem.at[1], core_peer)
     halo = lambda where: remote(halo_out, halo_in, halo_sem.at[0], halo_sem.at[1], {"sp": where})
 
     @pl.when(me < count - 1)
     def _():
         halo(me + 1).start()
 
+    for copy in stats[0]:
+        copy.start()
     w_swap.start()
-    convolve(halo_rows, tok_rows - halo_rows)
 
     @pl.when(me == 0)
     def _():
@@ -329,59 +364,54 @@
         padded_ref[:halo_rows, :] = halo_in[...].astype(f32)
 
     convolve(0, halo_rows)
-
-    conv_out = conv_ref[...]
-    diagonal = lax.broadcasted_iota(jnp.int32, (tok_rows, tok_rows), 0) == lax.broadcasted_iota(
-        jnp.int32, (tok_rows, tok_rows), 1
-    )
-
-    def lying(column):
-        return jnp.sum(jnp.where(diagonal, column, 0.0), axis=0, keepdims=True)
-
-    def standing(line):
-        return jnp.sum(jnp.where(diagonal, line, 0.0), axis=1, keepdims=True)
-
-    stat_out[0:1, :] = lying(jnp.sum(conv_out, axis=1, keepdims=True))
-    stat_out[1:2, :] = lying(jnp.sum(conv_out * conv_out, axis=1, keepdims=True))
-    stats = [
-        remote(stat_out, stat_in.at[at], stat_send.at[at], stat_recv.at[at], peer)
-        for at, peer in enumerate((core_peer, row_peer, far_peer))
-    ]
-    for copy in stats:
+    measure(0, halo_rows, 1)
+    for copy in stats[1]:
         copy.start()
     for load in loads[4:9]:
         load.wait()
-    for copy in stats:
-        copy.wait_recv()
-    sums = (stat_out[...] + stat_in[0]) + (stat_in[1] + stat_in[2])
-    channel_mean = standing(sums[0:1]) / channels_all
-    channel_var = standing(sums[1:2]) / channels_all - channel_mean * channel_mean
-    scaled = (conv_out - channel_mean) * lax.rsqrt(channel_var + LN_EPS) * ln_gain_ref[
-        ...
-    ] + ln_bias_ref[...]
-    mix_out[...] = silu(scaled).astype(bf16)
 
     def cut(at):
         return pl.ds(at * cut_rows, cut_rows)
 
-    mix = remote(mix_out, mix_in, mix_sem.at[0], mix_sem.at[1], core_peer)
-    mix.start()
-    keep_ref[...] = jnp.dot(mix_out[...], w_out_ref[...], preferred_element_type=f32)
-    w_swap.wait_recv()
+    mixes = [
+        remote(
+            mix_out.at[some], mix_in.at[some], mix_sem.at[2 + part], mix_sem.at[4 + part], core_peer
+        )
+        for part, some in enumerate((pl.ds(halo_rows, rest), pl.ds(0, halo_rows)))
+    ]
     chips = [
         remote(
             chip_out.at[cut(at)], chip_in.at[cut(at)], chip_send.at[at], chip_recv.at[at], row_peer
         )
         for at in range(ROW_CUTS)
     ]
-    mix.wait_recv()
-    for at in range(ROW_CUTS):
-        chip_sum = keep_ref[cut(at), :] + jnp.dot(
-            mix_in[cut(at), :], w_in[...], preferred_element_type=f32
-        )
-        keep_ref[cut(at), :] = chip_sum
-        chip_out[cut(at), :] = chip_sum.astype(bf16)
-        chips[at].start()
+
+    def project(first, size, part):
+        some = slice(first, first + size)
+        for copy in stats[part]:
+            copy.wait_recv()
+        sums = (stat_out[part] + stat_in[part, 0]) + (stat_in[part, 1] + stat_in[part, 2])
+        channel_mean = standing(sums[0:1], first, size) / channels_all
+        channel_var = standing(sums[1:2], first, size) / channels_all - channel_mean * channel_mean
+        scaled = (conv_ref[some, :] - channel_mean) * lax.rsqrt(channel_var + LN_EPS) * ln_gain_ref[
+            ...
+        ] + ln_bias_ref[...]
+        mix_out[some, :] = silu(scaled).astype(bf16)
+        mixes[part].start()
+        keep_ref[some, :] = jnp.dot(mix_out[some, :], w_out_ref[...], preferred_element_type=f32)
+        if part == 0:
+            w_swap.wait_recv()
+        mixes[part].wait_recv()
+        for at in range((first + size) // cut_rows - 1, first // cut_rows - 1, -1):
+            chip_sum = keep_ref[cut(at), :] + jnp.dot(
+                mix_in[cut(at), :], w_in[...], preferred_element_type=f32
+            )
+            keep_ref[cut(at), :] = chip_sum
+            chip_out[cut(at), :] = chip_sum.astype(bf16)
+            chips[at].start()
+
+    project(halo_rows, rest, 0)
+    project(0, halo_rows, 1)
 
     def block(half, at, piece):
         return rows_ref.at[half, at, cut(piece)]
@@ -442,20 +472,19 @@
         normed_ref[some, :half_width] = (low * inverse * ffn_gain_ref[:, :half_width]).astype(bf16)
         normed_ref[some, half_width:] = (high * inverse * ffn_gain_ref[:, half_width:]).astype(bf16)
 
-    def far_copy(at, piece):
-        spot = hidden_ref.at[tp_place, at, cut(piece)]
-        sem = at * ROW_CUTS + piece
-        return remote(spot, spot, far_send.at[sem], far_recv.at[sem], row_peer)
-
-    def near_copy(at, piece):
-        spot = hidden_ref.at[tp_place, at, cut(piece)]
-        sem = at * ROW_CUTS + piece
-        return remote(spot, spot, near_send.at[sem], near_recv.at[sem], core_peer)
-
-    def relay_copy(at, piece):
-        spot = hidden_ref.at[row_place, at, cut(piece)]
-        sem = at * ROW_CUTS + piece
-        return remote(spot, spot, relay_send.at[sem], relay_recv.at[sem], core_peer)
+    def hidden_copy(place, at, run, send, recv, peer):
+        spot = hidden_ref.at[place, at, pl.ds(*run)]
+        sem = at * ROW_CUTS + run[0] // cut_rows
+        return remote(spot, spot, send.at[sem], recv.at[sem], peer)
+
+    def far_copy(at, run):
+        return hidden_copy(tp_place, at, run, far_send, far_recv, row_peer)
+
+    def near_copy(at, run):
+        return hidden_copy(tp_place, at, run, near_send, near_recv, core_peer)
+
+    def relay_copy(at, run):
+        return hidden_copy(row_place, at, run, relay_send, relay_recv, core_peer)
 
     shared_far = remote(
         shared_ref.at[tp_place], shared_ref.at[tp_place], shared_send.at[0], shared_recv.at[0], row_peer
@@ -467,27 +496,31 @@
         shared_ref.at[row_place], shared_ref.at[row_place], shared_send.at[2], shared_recv.at[2], core_peer
     )
 
-    every = range(ROW_CUTS)
-
-    def hide(at, pieces):
-        some = pl.ds(pieces[0] * cut_rows, len(pieces) * cut_rows)
-        for piece in pieces:
-            crossed(at, piece)
+    half_rows = tok_rows // 2
+    falling = range(ROW_CUTS - 1, -1, -1)
+    opening = (half_rows, half_rows)
+    closing = (0, half_rows)
+    halves = (opening, closing)
+    singles = tuple((piece * cut_rows, cut_rows) for piece in falling[: ROW_CUTS // 2])
+
+    def hide(at, first, size, runs):
+        some = pl.ds(first, size)
         normalise(at, some)
-        hide_rows(at, pieces)
-
-    def hide_rows(at, pieces):
-        some = pl.ds(pieces[0] * cut_rows, len(pieces) * cut_rows)
         step = 256
-        for first in range(0, part_hidden, step):
-            wide = slice(first, first + step)
+        for left in range(0, part_hidden, step):
+            wide = slice(left, left + step)
             gate_part = jnp.dot(normed_ref[some, :], gate_ref[:, wide], preferred_element_type=f32)
             up_part = jnp.dot(normed_ref[some, :], up_ref[:, wide], preferred_element_type=f32)
             hidden_ref[tp_place, at, some, wide] = (silu(gate_part) * up_part).astype(bf16)
-        for piece in pieces:
-            far_copy(at, piece).start()
-        for piece in pieces:
-            near_copy(at, piece).start()
+        for run in runs:
+            far_copy(at, run).start()
+        for run in runs:
+            near_copy(at, run).start()
+
+    def gather_hide(at, first, size, runs):
+        for piece in range((first + size) // cut_rows - 1, first // cut_rows - 1, -1):
+            crossed(at, piece)
+        hide(at, first, size, runs)
 
     def down_part(at, some, place):
         return jnp.dot(
@@ -496,33 +529,34 @@
             preferred_element_type=f32,
         )
 
-    def back_copy(at, piece):
+    def back_copy(at, half):
+        some = pl.ds(half * half_rows, half_rows)
         return remote(
-            part_ref.at[at, cut(piece)],
-            back_ref.at[me, cut(piece)],
-            back_send.at[at * ROW_CUTS + piece],
-            back_recv.at[me * ROW_CUTS + piece],
+            part_ref.at[at, some],
+            back_ref.at[me, some],
+            back_send.at[at * 2 + half],
+            back_recv.at[me * 2 + half],
             {"sp": at},
         )
 
-    def relay(at, piece):
-        far_copy(at, piece).wait_recv()
-        relay_copy(at, piece).start()
-
-    def finish(at, pieces):
-        for piece in pieces:
-            relay(at, piece)
-        for piece in pieces:
-            near_copy(at, piece).wait_recv()
-        for piece in pieces:
-            relay_copy(at, piece).wait_recv()
-        some = pl.ds(pieces[0] * cut_rows, len(pieces) * cut_rows)
+    def relay(at, run):
+        far_copy(at, run).wait_recv()
+        relay_copy(at, run).start()
+
+    def finish(at, first, size, runs):
+        for run in runs:
+            relay(at, run)
+        for run in runs:
+            near_copy(at, run).wait_recv()
+        for run in runs:
+            relay_copy(at, run).wait_recv()
+        some = pl.ds(first, size)
         total = (down_part(at, some, 0) + down_part(at, some, 1)) + (
             down_part(at, some, 2) + down_part(at, some, 3)
         )
         part_ref[at, some, :] = total.astype(bf16)
-        for piece in pieces:
-            back_copy(at, piece).start()
+        for half in range((first + size) // half_rows - 1, first // half_rows - 1, -1):
+            back_copy(at, half).start()
 
     def pass_on(step, piece):
         below = level - step
@@ -551,7 +585,7 @@
             core_copy(above * 2 + side, piece).start()
 
     def from_side(at):
-        for piece in every:
+        for piece in falling:
             landed(at, piece)
             core_copy(at, piece).start()
 
@@ -560,63 +594,70 @@
 
     def visited(outer_way, inner_way):
         mirrored = outer_way[0] + inner * (inner_way[0] - outer_way[0])
-        other = outer_way[1] + inner * (inner_way[1] - outer_way[1])
         at_level = mirrored + upper * (levels - 1 - 2 * mirrored)
-        return at_level * 2 + lax.rem(side + other, 2), other
-
-    outer_order = ((0, 1), (1, 0), (2, 0), (3, 0), (2, 1), (3, 1), (1, 1))
-    inner_order = ((0, 0), (2, 0), (3, 0), (2, 1), (0, 1), (3, 1), (1, 1))
-    visits = [visited(*ways) for ways in zip(outer_order, inner_order)]
-
-    settle(0)
-    for load in loads[9:13]:
-        load.wait()
-    hide(me, (0,))
-    settle(1)
-    first = visits[0][0]
+        return at_level * 2 + lax.rem(side + outer_way[1], 2)
+
+    outer_order = ((1, 0), (2, 0), (3, 0), (2, 1), (3, 1), (1, 1))
+    inner_order = ((0, 0), (2, 0), (3, 0), (2, 1), (0, 1), (3, 1))
+    next_door, *visits = [visited(*ways) for ways in zip(outer_order, inner_order)]
     beside = level * 2 + (1 - side)
-    for piece in every:
+
+    def forward(piece):
         landed(beside, piece)
         core_copy(beside, piece).start()
         pass_on(1, piece)
-        hide(first, (piece,))
-    for load in loads[13:]:
+
+    settle(falling[0])
+    settle(falling[1])
+    for load in loads[9:11]:
         load.wait()
-    hide(visits[1][0], every)
-    for piece in every:
+    gather_hide(me, *singles[0], singles[:1])
+    settle(falling[2])
+    forward(falling[0])
+    gather_hide(me, *singles[1], singles[1:])
+    settle(falling[3])
+    forward(falling[1])
+    gather_hide(next_door, *singles[0], singles[:1])
+    gather_hide(next_door, *singles[1], singles[1:])
+    forward(falling[2])
+    gather_hide(beside, *opening, (opening,))
+    forward(falling[3])
+    gather_hide(next_door, *closing, (closing,))
+    for load in loads[11:]:
+        load.wait()
+    for piece in falling:
         pass_on(2, piece)
-    relay(me, 0)
+    gather_hide(visits[0], 0, tok_rows, halves)
+    for piece in falling:
+        pass_on(3, piece)
+    gather_hide(visits[1], 0, tok_rows, halves)
+    from_side(visits[2])
+    for run in singles:
+        relay(me, run)
+    finish(next_door, 0, tok_rows, singles + (closing,))
+    gather_hide(visits[2], 0, tok_rows, halves)
+    from_side(visits[3])
+    finish(beside, *opening, (opening,))
+    finish(visits[0], 0, tok_rows, halves)
+    gather_hide(visits[3], 0, tok_rows, halves)
+    from_side(visits[4])
+    finish(visits[1], 0, tok_rows, halves)
+
+    for piece in falling[2:]:
+        crossed(me, piece)
     whole = pl.ds(0, tok_rows)
-
-    def fetch(turn):
-        at, other = visits[turn]
-
-        @pl.when(other == 1)
-        def _():
-            @pl.when(at != beside)
-            def _():
-                from_side(at)
-
-    for turn in range(2, len(visits)):
-        at = visits[turn][0]
-        hide(at, every)
-        if turn + 1 < len(visits):
-            fetch(turn + 1)
-        finish(visits[turn - 2][0], every)
-        if turn == 2:
-            for piece in every:
-                pass_on(3, piece)
-        if turn == 4:
-            crossed(me, 1)
-            normalise(me, whole)
-            shared_gate = jnp.dot(normed_ref[...], sh_gate_ref[...], preferred_element_type=f32)
-            shared_up = jnp.dot(normed_ref[...], sh_up_ref[...], preferred_element_type=f32)
-            shared_ref[tp_place] = (silu(shared_gate) * shared_up).astype(bf16)
-            shared_far.start()
-            shared_near.start()
-
-    normalise(me, cut(1))
-    hide_rows(me, (1,))
+    normalise(me, whole)
+    shared_gate = jnp.dot(normed_ref[...], sh_gate_ref[...], preferred_element_type=f32)
+    shared_up = jnp.dot(normed_ref[...], sh_up_ref[...], preferred_element_type=f32)
+    shared_ref[tp_place] = (silu(shared_gate) * shared_up).astype(bf16)
+    shared_far.start()
+    shared_near.start()
+
+    gather_hide(visits[4], 0, tok_rows, halves)
+    finish(visits[2], 0, tok_rows, halves)
+    gather_hide(beside, *closing, (closing,))
+    hide(me, *closing, (closing,))
+
     middle_cols = rows_ref[row, me, :, pl.ds(pl.multiple_of(core * col_width, col_width), col_width)]
     shared_far.wait_recv()
     shared_relay.start()
@@ -631,43 +672,44 @@
             preferred_element_type=f32,
         )
     sum_ref[...] = total
-    finish(visits[-2][0], every)
-    for piece in every:
-        finish(visits[-1][0], (piece,))
-
-    for piece in every:
-        near_copy(me, piece).wait_recv()
-    relay_copy(me, 0).wait_recv()
+    finish(visits[3], 0, tok_rows, halves)
+    finish(visits[4], 0, tok_rows, halves)
+    finish(beside, *closing, (closing,))
+
+    for run in singles + (closing,):
+        near_copy(me, run).wait_recv()
+    for run in singles:
+        relay_copy(me, run).wait_recv()
     own_part = down_part(me, whole, tp_place) + down_part(me, whole, core_place)
-    relay(me, 1)
+    relay(me, closing)
     own_part = own_part + down_part(me, whole, row_place)
-    relay_copy(me, 1).wait_recv()
+    relay_copy(me, closing).wait_recv()
     own_part = own_part + down_part(me, whole, (1 - row) * 2 + (1 - core))
     part_ref[me] = own_part.astype(bf16)
     total = sum_ref[...]
     routes = routes_ref[...]
     route_weights = route_weights_ref[...]
-    own_weight = standing(jnp.sum(jnp.where(routes == me, route_weights, 0.0), axis=0, keepdims=True))
-    total = total + own_weight * part_ref[me].astype(f32)
+    def weight_of(at):
+        line = jnp.sum(jnp.where(routes == at, route_weights, 0.0), axis=0, keepdims=True)
+        return standing(line, 0, tok_rows)
+
+    total = total + weight_of(me) * part_ref[me].astype(f32)
     for step in range(1, count):
         at = lax.rem(me + step, count)
-        for piece in every:
+        for half in range(2):
+            some = pl.ds(half * half_rows, half_rows)
+            sem = at * 2 + half
             remote(
-                part_ref.at[at, cut(piece)],
-                back_ref.at[at, cut(piece)],
-                back_send.at[at * ROW_CUTS + piece],
-                back_recv.at[at * ROW_CUTS + piece],
-                core_peer,
+                part_ref.at[at, some], back_ref.at[at, some], back_send.at[sem], back_recv.at[sem], core_peer
             ).wait_recv()
-        weight = standing(jnp.sum(jnp.where(routes == at, route_weights, 0.0), axis=0, keepdims=True))
-        total = total + weight * back_ref[at].astype(f32)
+        total = total + weight_of(at) * back_ref[at].astype(f32)
     out_ref[...] = total.astype(bf16)
 
     @pl.when(me < count - 1)
     def _():
         halo(me + 1).wait_send()
 
-    for copy in stats + chips + [w_swap, mix, shared_far, shared_near, shared_relay]:
+    for copy in stats[0] + stats[1] + mixes + chips + [w_swap, shared_far, shared_near, shared_relay]:
         copy.wait_send()
 
     @pl.loop(0, levels)
@@ -683,18 +725,23 @@
             def _():
                 low_copy(origin, piece).wait_send()
 
+    split = singles + (closing,)
+    trips = [(me, split), (next_door, split), (beside, halves)] + [(at, halves) for at in visits]
+    for at, runs in trips:
+        for run in runs:
+            far_copy(at, run).wait_send()
+            near_copy(at, run).wait_send()
+            relay_copy(at, run).wait_send()
+
     @pl.loop(0, count)
     def _(at):
-        for piece in every:
+        for piece in range(ROW_CUTS):
             core_copy(at, piece).wait_send()
-            far_copy(at, piece).wait_send()
-            near_copy(at, piece).wait_send()
-            relay_copy(at, piece).wait_send()
 
         @pl.when(at != me)
         def _():
-            for piece in every:
-                back_copy(at, piece).wait_send()
+            for half in range(2):
+                back_copy(at, half).wait_send()
 
 
 def body_dense(
@@ -725,8 +772,7 @@
     col_width = exp_down.shape[2]
     shared_width = sh_gate.shape[1]
     top_count = routes.shape[1]
-    span = conv_kernel.shape[0]
-    halo_rows = -(-(span - 1) // 16) * 16
+    halo_rows = tok_rows // ROW_CUTS
     vmem = pl.BlockSpec(memory_space=pltpu.VMEM)
     hbm = pl.BlockSpec(memory_space=pltpu.HBM)
     f32, bf16 = jnp.float32, jnp.bfloat16
@@ -778,8 +824,8 @@
             pltpu.VMEM((halo_rows, channels), bf16),
             pltpu.VMEM((halo_rows + tok_rows, channels), f32),
             pltpu.VMEM((tok_rows, channels), f32),
-            pltpu.VMEM((2, tok_rows), f32),
-            pltpu.VMEM((3, 2, tok_rows), f32),
+            pltpu.VMEM((2, 2, tok_rows), f32),
+            pltpu.VMEM((2, 3, 2, tok_rows), f32),
             pltpu.VMEM((tok_rows, channels), bf16),
             pltpu.VMEM((tok_rows, channels), bf16),
             pltpu.VMEM((channels, half_width), bf16),
@@ -795,9 +841,9 @@
             pltpu.VMEM((tok_rows, col_width), f32),
             dma((17,)),
             dma((2,)),
-            dma((3,)),
-            dma((3,)),
-            dma((4,)),
+            dma((6,)),
+            dma((6,)),
+            dma((6,)),
             dma((ROW_CUTS,)),
             dma((ROW_CUTS,)),
             dma((levels * ROW_CUTS,)),
@@ -814,8 +860,8 @@
             dma((pieces,)),
             dma((3,)),
             dma((3,)),
-            dma((pieces,)),
-            dma((pieces,)),
+            dma((2 * count,)),
+            dma((2 * count,)),
         ],
         compiler_params=pltpu.CompilerParams(
             collective_id=0, has_side_effects=True, vmem_limit_bytes=56 * 1024 * 1024
@@ -833,6 +879,7 @@
         local_experts == 1
         and lax.axis_size("tp") == 4
         and lax.axis_size("sp") == 8
+        and ROW_CUTS * (args[3].shape[0] - 1) <= tok_rows
         and capacity >= tok_rows
     ):
         return body_dense(*args)

time: 77.8 us -> 78.8 us (1.013)
  Pallas kernels: 76 us -> 77.1 us
    pallas_call x1, Pallas kernels: 76 us -> 77.1 us  [body_dense(): pl.pallas_call(functools.partial(layer_kernel, levels), out_shape=jax.Sha...]
where the time goes in v4:
time: 78.8 us; the launch traced here: 78.7 us
  Pallas kernels  77.1 us (98%)
  local copies, waits for them, and re-layouts  1.57 us (2%)
    pallas_call x1, Pallas kernels, body_dense(): pl.pallas_call(functools.partial(layer_kernel, levels), out_shape=jax.Sha...  77.1 us

profile of v4, /device:TPU:0, one launch (start us, length us, event | category | flops | bytes accessed | tf_op | source)
XLA Modules:
  0.0 78.7 jit_solution(17556710274019111311)
XLA Ops:
  0.0 77.1 %shard_map.163 = bf16[128,512]{1,0:T(8,128)(2,1)} custom-call(bf16[128,2048]{1,0:T(8,128)(2,1)} %resid_hbm.1, bf16[128,256]{1,0:T(8,128)(2,1)} %a_val_hbm.1, bf16[128,256]{1,0:T(8,128)(2,1)} %a_gate_hbm.1, bf16[31,256]{1,0:T(8,128)(2,1)} %taps_hbm.1, f32[1,256]{1,0:T(1,128)} %bitcast.15, f32[1,256]{1,0:T(1,128)} %bitcast.16, f32[1,256]{1,0:T(1,128)} %bitcast.17, ...), custom_call_target="tpu_custom_call" | custom-call | tf_op jit(solution)/shard_map/pallas_call | solution.py:800
  77.1 1.6 %copy.19 = bf16[128,512]{1,0:T(8,128)(2,1)} copy(bf16[128,512]{1,0:T(8,128)(2,1)} %shard_map.163) | data formatting | bytes 262144

commit v5 on v4

--- a/solution.py
+++ b/solution.py
@@ -129,7 +129,8 @@
     return (middle_cols.astype(jnp.float32) + shared + routed).astype(jnp.bfloat16)
 
 
-ROW_CUTS = 4
+ROW_CUTS = 2
+HALO_PART = 4
 
 
 def silu(value):
@@ -192,6 +193,7 @@
     part_ref,
     back_ref,
     sum_ref,
+    weight_ref,
     load_sem,
     halo_sem,
     stat_send,
@@ -386,7 +388,7 @@
         for at in range(ROW_CUTS)
     ]
 
-    def project(first, size, part):
+    def project(first, size, part, sending):
         some = slice(first, first + size)
         for copy in stats[part]:
             copy.wait_recv()
@@ -402,7 +404,7 @@
         if part == 0:
             w_swap.wait_recv()
         mixes[part].wait_recv()
-        for at in range((first + size) // cut_rows - 1, first // cut_rows - 1, -1):
+        for at in sending:
             chip_sum = keep_ref[cut(at), :] + jnp.dot(
                 mix_in[cut(at), :], w_in[...], preferred_element_type=f32
             )
@@ -410,8 +412,8 @@
             chip_out[cut(at), :] = chip_sum.astype(bf16)
             chips[at].start()
 
-    project(halo_rows, rest, 0)
-    project(0, halo_rows, 1)
+    project(halo_rows, rest, 0, range(ROW_CUTS - 1, 0, -1))
+    project(0, halo_rows, 1, (0,))
 
     def block(half, at, piece):
         return rows_ref.at[half, at, cut(piece)]
@@ -608,29 +610,21 @@
         pass_on(1, piece)
 
     settle(falling[0])
-    settle(falling[1])
     for load in loads[9:11]:
         load.wait()
-    gather_hide(me, *singles[0], singles[:1])
-    settle(falling[2])
+    gather_hide(me, *opening, (opening,))
+    settle(falling[1])
     forward(falling[0])
-    gather_hide(me, *singles[1], singles[1:])
-    settle(falling[3])
+    gather_hide(next_door, *opening, (opening,))
     forward(falling[1])
-    gather_hide(next_door, *singles[0], singles[:1])
-    gather_hide(next_door, *singles[1], singles[1:])
-    forward(falling[2])
     gather_hide(beside, *opening, (opening,))
-    forward(falling[3])
     gather_hide(next_door, *closing, (closing,))
-    for load in loads[11:]:
+    for step, at in ((2, visits[0]), (3, visits[1])):
+        for piece in falling:
+            pass_on(step, piece)
+        gather_hide(at, 0, tok_rows, halves)
+    for load in loads[11:15]:
         load.wait()
-    for piece in falling:
-        pass_on(2, piece)
-    gather_hide(visits[0], 0, tok_rows, halves)
-    for piece in falling:
-        pass_on(3, piece)
-    gather_hide(visits[1], 0, tok_rows, halves)
     from_side(visits[2])
     for run in singles:
         relay(me, run)
@@ -643,7 +637,7 @@
     from_side(visits[4])
     finish(visits[1], 0, tok_rows, halves)
 
-    for piece in falling[2:]:
+    for piece in falling[1:]:
         crossed(me, piece)
     whole = pl.ds(0, tok_rows)
     normalise(me, whole)
@@ -652,6 +646,14 @@
     shared_ref[tp_place] = (silu(shared_gate) * shared_up).astype(bf16)
     shared_far.start()
     shared_near.start()
+
+    for load in loads[15:]:
+        load.wait()
+    for at in range(count):
+        line = jnp.sum(
+            jnp.where(routes_ref[...] == at, route_weights_ref[...], 0.0), axis=0, keepdims=True
+        )
+        weight_ref[at] = jnp.broadcast_to(standing(line, 0, tok_rows), weight_ref.shape[1:])
 
     gather_hide(visits[4], 0, tok_rows, halves)
     finish(visits[2], 0, tok_rows, halves)
@@ -673,8 +675,22 @@
         )
     sum_ref[...] = total
     finish(visits[3], 0, tok_rows, halves)
-    finish(visits[4], 0, tok_rows, halves)
+    for half in halves:
+        finish(visits[4], *half, (half,))
     finish(beside, *closing, (closing,))
+
+    def add(at, rows):
+        weight = jnp.concatenate([weight_ref[at]] * (col_width // weight_ref.shape[2]), axis=1)
+        sum_ref[...] += weight * rows.astype(f32)
+
+    def add_back(at):
+        for half in range(2):
+            some = pl.ds(half * half_rows, half_rows)
+            sem = at * 2 + half
+            remote(
+                part_ref.at[at, some], back_ref.at[at, some], back_send.at[sem], back_recv.at[sem], core_peer
+            ).wait_recv()
+        add(at, back_ref[at])
 
     for run in singles + (closing,):
         near_copy(me, run).wait_recv()
@@ -683,26 +699,13 @@
     own_part = down_part(me, whole, tp_place) + down_part(me, whole, core_place)
     relay(me, closing)
     own_part = own_part + down_part(me, whole, row_place)
+    for step in range(2, count):
+        add_back(lax.rem(level * 2 + step, count))
     relay_copy(me, closing).wait_recv()
     own_part = own_part + down_part(me, whole, (1 - row) * 2 + (1 - core))
-    part_ref[me] = own_part.astype(bf16)
+    add(me, own_part.astype(bf16))
+    add_back(beside)
     total = sum_ref[...]
-    routes = routes_ref[...]
-    route_weights = route_weights_ref[...]
-    def weight_of(at):
-        line = jnp.sum(jnp.where(routes == at, route_weights, 0.0), axis=0, keepdims=True)
-        return standing(line, 0, tok_rows)
-
-    total = total + weight_of(me) * part_ref[me].astype(f32)
-    for step in range(1, count):
-        at = lax.rem(me + step, count)
-        for half in range(2):
-            some = pl.ds(half * half_rows, half_rows)
-            sem = at * 2 + half
-            remote(
-                part_ref.at[at, some], back_ref.at[at, some], back_send.at[sem], back_recv.at[sem], core_peer
-            ).wait_recv()
-        total = total + weight_of(at) * back_ref[at].astype(f32)
     out_ref[...] = total.astype(bf16)
 
     @pl.when(me < count - 1)
@@ -772,7 +775,7 @@
     col_width = exp_down.shape[2]
     shared_width = sh_gate.shape[1]
     top_count = routes.shape[1]
-    halo_rows = tok_rows // ROW_CUTS
+    halo_rows = tok_rows // HALO_PART
     vmem = pl.BlockSpec(memory_space=pltpu.VMEM)
     hbm = pl.BlockSpec(memory_space=pltpu.HBM)
     f32, bf16 = jnp.float32, jnp.bfloat16
@@ -839,6 +842,7 @@
             pltpu.VMEM((count, tok_rows, col_width), bf16),
             pltpu.VMEM((count, tok_rows, col_width), bf16),
             pltpu.VMEM((tok_rows, col_width), f32),
+            pltpu.VMEM((count, tok_rows, 128), f32),
             dma((17,)),
             dma((2,)),
             dma((6,)),
@@ -879,7 +883,7 @@
         local_experts == 1
         and lax.axis_size("tp") == 4
         and lax.axis_size("sp") == 8
-        and ROW_CUTS * (args[3].shape[0] - 1) <= tok_rows
+        and HALO_PART * (args[3].shape[0] - 1) <= tok_rows
         and capacity >= tok_rows
     ):
         return body_dense(*args)

time: 78.8 us -> 75.2 us (0.954)
  Pallas kernels: 77.1 us -> 73.5 us
    pallas_call x1, Pallas kernels: 77.1 us -> 73.5 us  [body_dense(): pl.pallas_call(functools.partial(layer_kernel, levels), out_shape=jax.Sha...]
where the time goes in v5:
time: 75.2 us; the launch traced here: 75.1 us
  Pallas kernels  73.5 us (98%)
  local copies, waits for them, and re-layouts  1.57 us (2%)
    pallas_call x1, Pallas kernels, body_dense(): pl.pallas_call(functools.partial(layer_kernel, levels), out_shape=jax.Sha...  73.5 us
    unnamed x1, local copies, waits for them, and re-layouts  1.57 us

profile of v5, /device:TPU:0, one launch (start us, length us, event | category | flops | bytes accessed | tf_op | source)
XLA Modules:
  0.0 75.1 jit_solution(7923887801884264997)
XLA Ops:
  0.0 73.5 %shard_map.163 = bf16[128,512]{1,0:T(8,128)(2,1)} custom-call(bf16[128,2048]{1,0:T(8,128)(2,1)} %resid_hbm.1, bf16[128,256]{1,0:T(8,128)(2,1)} %a_val_hbm.1, bf16[128,256]{1,0:T(8,128)(2,1)} %a_gate_hbm.1, bf16[31,256]{1,0:T(8,128)(2,1)} %taps_hbm.1, f32[1,256]{1,0:T(1,128)} %bitcast.15, f32[1,256]{1,0:T(1,128)} %bitcast.16, f32[1,256]{1,0:T(1,128)} %bitcast.17, ...), custom_call_target="tpu_custom_call" | custom-call | tf_op jit(solution)/shard_map/pallas_call | solution.py:803
  73.5 1.6 %copy.19 = bf16[128,512]{1,0:T(8,128)(2,1)} copy(bf16[128,512]{1,0:T(8,128)(2,1)} %shard_map.163) | data formatting | bytes 262144
